TPU v7x, 32 devices: a whole 2x2x4 slice. The times are simulated.
32 devices in a mesh: sp: 4 (over z), fs: 4 (over y, x), tp: 2 (over core).
Axes of the slice: x: 2, y: 2, z: 4, core: 2. Of those that a mesh axis runs over, the one named last changes fastest.
Arguments:
- tokens: bfloat16 [8, 1536, 2048], P('fs', ('sp', 'tp')), may hold values from -6 to 6
- norm_gain: float32 [2048], replicated, may hold values from 0.1 to 1.9
- chain_entry: bfloat16 [2048, 2048], P(('sp', 'fs'), 'tp'), may hold values from -0.125 to 0.125
- pool_entry: bfloat16 [2048, 2048], P(('sp', 'fs'), 'tp'), may hold values from -0.125 to 0.125
- conv_taps: bfloat16 [4, 2048], P(None, 'tp'), may hold values from -3 to 3
- recur_gate: bfloat16 [8, 256, 256], P('tp'), may hold values from -0.375 to 0.375
- input_gate: bfloat16 [8, 256, 256], P('tp'), may hold values from -0.375 to 0.375
- decay_log: float32 [2048], P('tp'), may hold values from -9 to 5
- decay_shift: float32 [8, 1536, 2048], P('fs', 'sp', 'tp'), may hold values from -1 to 0
- start_state: float32 [8, 2048], P('fs', 'tp'), may hold values from -6 to 6
- pool_mix: bfloat16 [8, 256, 256], P('tp'), may hold values from -0.375 to 0.375
- pool_scale: float32 [2048], P('tp'), may hold values from 0.1 to 1.9
- chain_exit: bfloat16 [2048, 2048], P('tp', ('sp', 'fs')), may hold values from -0.09375 to 0.09375
- pool_exit: bfloat16 [2048, 2048], P('tp', ('sp', 'fs')), may hold values from -0.09375 to 0.09375
Outputs:
- mixed_rows: bfloat16 [8, 1536, 2048], P('fs', ('sp', 'tp'))
All inputs are finite; a program needn't handle non-finite values.
Results may differ from a plain program's by a relative error of at most 0.01.
Values may be sent and summed in bfloat16 or wider, within the bound.
A program may use at most 128 MiB of HBM per device.

v0:
```python
import functools

import jax
import jax.numpy as jnp
from jax import lax
from jax.experimental import pallas as pl
from jax.experimental.pallas import tpu as pltpu
from jax.sharding import PartitionSpec as P

MESH = pl.DeviceIdType.MESH
NORM_EPSILON = 1e-06
RECUR_SCALE = 8.0
HALO = 16
COLS = 256
ROWS = 64
F32 = jnp.float32
BF16 = jnp.bfloat16


def neg_expm1(x):
    y = -x
    poly = 1.0 - y * (1.0 / 9.0)
    for k in range(8, 1, -1):
        poly = 1.0 - y * (1.0 / k) * poly
    return jnp.where(y < 0.5, y * poly, 1.0 - jnp.exp(x))


def kernel(
    n, m,
    tokens, gain, chain_entry, pool_entry, taps, rgate, igate, dlog, shift_hbm, start,
    pmix, pscale, chain_exit, pool_exit,
    out,
    w0, w1, w2, w3, raw, normed, cbuf, pbuf, shift, rg, ig, pm,
    convb, zr, zi, cum_a, cum_b, rec, pooled, my_ab, all_ab, ent, acc, sendbuf, recvbuf,
    s1, r1, s2, r2, t1s, t1r, t2s, t2r, loc, nsem, hsem_s, hsem_r, ab_s, ab_r, out_s, out_r,
):
    sp, fs, tp = lax.axis_index("sp"), lax.axis_index("fs"), lax.axis_index("tp")
    shards = (chain_entry, pool_entry, chain_exit, pool_exit)
    bufs = (w0, w1, w2, w3)
    seqs, half_rows, width = raw.shape
    rows = 2 * half_rows
    chans = cbuf.shape[2]
    nb = chans // COLS
    far = m // 2
    full = (m - 1) // 2

    def ring(i):
        return i + (i // 2) * (5 - 2 * i) if m == 4 else i

    pos = ring(fs)
    right, left = ring((pos + 1) % m), ring((pos + m - 1) % m)

    barrier = pltpu.get_barrier_semaphore()
    greet = [{"sp": (sp + k) % n} for k in range(1, n)] + [{"tp": 1 - tp}]
    greet += [{"fs": ring((pos + k) % m)} for k in range(1, m)]
    for device in greet:
        pl.semaphore_signal(barrier, inc=1, device_id=device, device_id_type=MESH)

    def span(w, part):
        block = shards[w].shape[0]
        tail = block // 8 // 16 * 16
        head = block - tail
        cut = -(-head // 32) * 16
        if w % 2:
            cut = head - cut
        return {"all": (0, block), None: (0, head), 0: (0, cut), 1: (cut, head - cut),
                2: (head, tail)}[part]

    def region(w, p, q, part=None):
        lo, size = span(w, part)
        at = (((sp + p) % n) * m + ring((pos + q + m) % m)) * shards[w].shape[0] + lo
        return bufs[w].at[pl.ds(pl.multiple_of(at, 16), size)]

    def own(w, part=None):
        lo, size = span(w, part)
        return shards[w].at[pl.ds(lo, size)]

    has_tail = span(0, 2)[1] > 0 and m > 1

    started = []

    def launch(copy):
        copy.start()
        started.append(copy)

    def first(w, k):
        return pltpu.make_async_remote_copy(
            src_ref=own(w), dst_ref=region(w, 0, 0), send_sem=s1.at[w * n + k],
            recv_sem=r1.at[w * n + n - k], device_id={"sp": (sp + k) % n}, device_id_type=MESH)

    def first_wait(w, p):
        pltpu.make_async_remote_copy(
            src_ref=own(w), dst_ref=region(w, p, 0), send_sem=s1.at[w * n + p],
            recv_sem=r1.at[w * n + p], device_id={"sp": (sp + p) % n},
            device_id_type=MESH).wait_recv()

    def second(w, p, way, d):
        q = -d if way == 0 else d
        part = way if (m % 2 == 0 and d + 1 == far) else None
        if p == 0 and d == 0:
            src = own(w, part)
        else:
            src = region(w, p, q, part)
        at = ((w * n + p) * 2 + way) * max(far, 1) + d
        return pltpu.make_async_remote_copy(
            src_ref=src, dst_ref=region(w, p, q, part), send_sem=s2.at[at], recv_sem=r2.at[at],
            device_id={"fs": right if way == 0 else left}, device_id_type=MESH)

    def second_wait(w, p, way, d):
        q = -d if way == 0 else d
        part = way if (m % 2 == 0 and d == far) else None
        at = ((w * n + p) * 2 + way) * max(far, 1) + d - 1
        ref = region(w, p, q, part)
        pltpu.make_async_remote_copy(
            src_ref=ref, dst_ref=ref, send_sem=s2.at[at], recv_sem=r2.at[at],
            device_id={"fs": right if way == 0 else left}, device_id_type=MESH).wait_recv()

    def second_all(w, p):
        if far >= 1:
            for way in (0, 1):
                launch(second(w, p, way, 0))

    def forward(w, p):
        for d in range(1, far):
            for way in (0, 1):
                second_wait(w, p, way, d)
                launch(second(w, p, way, d))

    def last_wait(w, p):
        tail_wait(w, p)
        if far >= 1:
            for way in (0, 1):
                second_wait(w, p, way, far)

    def tail_one(w, k):
        return pltpu.make_async_remote_copy(
            src_ref=own(w, 2), dst_ref=region(w, 0, 0, 2), send_sem=t1s.at[w * m + k],
            recv_sem=t1r.at[w * m + m - k], device_id={"fs": ring((pos + k) % m)},
            device_id_type=MESH)

    def tail_one_wait(w, q):
        ref = region(w, 0, q, 2)
        pltpu.make_async_remote_copy(
            src_ref=ref, dst_ref=ref, send_sem=t1s.at[w * m + q], recv_sem=t1r.at[w * m + q],
            device_id={"fs": ring((pos + q) % m)}, device_id_type=MESH).wait_recv()

    def tail_two(w, q, k):
        at = (w * m + q) * n
        return pltpu.make_async_remote_copy(
            src_ref=own(w, 2) if q == 0 else region(w, 0, q, 2), dst_ref=region(w, 0, q, 2),
            send_sem=t2s.at[at + k], recv_sem=t2r.at[at + n - k],
            device_id={"sp": (sp + k) % n}, device_id_type=MESH)

    def tail_start(w):
        if has_tail:
            for k in range(1, m):
                launch(tail_one(w, k))

    def tail_forward(w):
        if has_tail:
            for q in range(m):
                if q:
                    tail_one_wait(w, q)
                for k in order:
                    launch(tail_two(w, q, k))

    def tail_wait(w, p):
        if has_tail and p:
            for q in range(m):
                ref = region(w, p, q, 2)
                at = (w * m + q) * n + p
                pltpu.make_async_remote_copy(
                    src_ref=ref, dst_ref=ref, send_sem=t2s.at[at], recv_sem=t2r.at[at],
                    device_id={"sp": (sp + p) % n}, device_id_type=MESH).wait_recv()

    order = sorted(range(1, n), key=lambda p: min(p, n - p))
    local = [
        pltpu.make_async_copy(tokens, raw, loc.at[0]),
        pltpu.make_async_copy(shift_hbm, shift, loc.at[1]),
        pltpu.make_async_copy(rgate, rg, loc.at[2]),
        pltpu.make_async_copy(igate, ig, loc.at[3]),
        pltpu.make_async_copy(pmix, pm, loc.at[4]),
    ] + [pltpu.make_async_copy(shards[w], region(w, 0, 0, "all"), loc.at[5 + w]) for w in range(4)]
    for copy in local:
        copy.start()

    pl.semaphore_wait(barrier, len(greet))
    for w in (0, 1):
        second_all(w, 0)
        for k in order:
            launch(first(w, k))
        tail_start(w)

    local[0].wait()
    mine = tp * half_rows

    def norm_step(i, c):
        s, r = i // (half_rows // ROWS), (i % (half_rows // ROWS)) * ROWS
        x = raw[s, pl.ds(pl.multiple_of(r, ROWS), ROWS), :].astype(F32)
        scale = lax.rsqrt(jnp.mean(x * x, axis=-1, keepdims=True) + NORM_EPSILON)
        normed[s, pl.ds(pl.multiple_of(mine + r, ROWS), ROWS), :] = (
            x * scale * gain[...]).astype(BF16)
        return c

    lax.fori_loop(0, seqs * (half_rows // ROWS), norm_step, 0)

    def normed_copy(owner):
        ref = normed.at[:, pl.ds(pl.multiple_of(owner * half_rows, ROWS), half_rows)]
        return pltpu.make_async_remote_copy(
            src_ref=ref, dst_ref=ref, send_sem=nsem.at[0], recv_sem=nsem.at[1],
            device_id={"tp": 1 - tp}, device_id_type=MESH)

    for p in order:
        for w in (0, 1):
            first_wait(w, p)
            second_all(w, p)
        if p == order[0]:
            launch(normed_copy(tp))
    for w in (0, 1):
        tail_forward(w)
    for w in (2, 3):
        for k in order:
            launch(first(w, k))
        tail_start(w)
    for p in [0] + order:
        for w in (0, 1):
            forward(w, p)
    for w in (2, 3):
        second_all(w, 0)
    for p in [0] + order:
        for w in (0, 1):
            last_wait(w, p)
    for p in order:
        for w in (2, 3):
            first_wait(w, p)
            second_all(w, p)
    for w in (2, 3):
        tail_forward(w)
    for copy in local[1:]:
        copy.wait()
    normed_copy(1 - tp).wait_recv()

    def lanes(c):
        return pl.ds(pl.multiple_of(c * COLS, COLS), COLS)

    def entry_step(i, c):
        s, b = i // nb, lanes(i % nb)
        x = normed[s]
        cbuf[s, HALO:, b] = jnp.dot(x, w0[:, b], preferred_element_type=F32).astype(BF16)
        pbuf[s, HALO:, b] = jnp.dot(x, w1[:, b], preferred_element_type=F32).astype(BF16)
        return c

    lax.fori_loop(0, seqs * nb, entry_step, 0)

    def halo(i, ref):
        return pltpu.make_async_remote_copy(
            src_ref=ref.at[:, rows:], dst_ref=ref.at[:, :HALO], send_sem=hsem_s.at[i],
            recv_sem=hsem_r.at[i], device_id={"sp": (sp + 1) % n}, device_id_type=MESH)

    todo = [(w, p) for p in [0] + order for w in (2, 3)]

    def some_forwards(count):
        for w, p in todo[:count]:
            forward(w, p)
        del todo[:count]

    some_forwards(2)

    @pl.when(sp < n - 1)
    def _():
        halo(0, cbuf).start()
        halo(1, pbuf).start()

    @pl.when(sp > 0)
    def _():
        halo(0, cbuf).wait_recv()
        halo(1, pbuf).wait_recv()

    @pl.when(sp == 0)
    def _():
        cbuf[:, :HALO, :] = jnp.zeros((seqs, HALO, chans), BF16)
        pbuf[:, :HALO, :] = jnp.zeros((seqs, HALO, chans), BF16)

    tap_count = taps.shape[0]
    inverse_length = 1.0 / (rows * n)

    def chain_step(g, s):
        b = lanes(g)
        tap = taps[:, b].astype(F32)

        def conv(i, c):
            r = pl.multiple_of(i * ROWS, ROWS)
            v = cbuf[s, pl.ds(r, ROWS + HALO), b].astype(F32)
            total = v * tap[tap_count - 1 : tap_count]
            for j in range(tap_count - 1):
                total = total + pltpu.roll(v, tap_count - 1 - j, 0) * tap[j : j + 1]
            convb[pl.ds(r, ROWS), :] = total[HALO:].astype(BF16)
            return c

        lax.fori_loop(0, rows // ROWS, conv, 0)
        x = convb[...]
        zr[...] = jnp.dot(x, rg[g], preferred_element_type=F32)
        zi[...] = jnp.dot(x, ig[g], preferred_element_type=F32)
        rate = -RECUR_SCALE * (jnp.exp(dlog[:, b]) * inverse_length)
        row = lax.broadcasted_iota(jnp.int32, (ROWS, COLS), 0)

        def scan(i, carry):
            r = pl.multiple_of(i * ROWS, ROWS)
            at = pl.ds(r, ROWS)
            log_decay = jax.nn.sigmoid(zr[at, :]) * rate + shift[s, at, b]
            a = jnp.exp(log_decay)
            d = (jnp.sqrt(neg_expm1(2.0 * log_decay)) * jax.nn.sigmoid(zi[at, :])
                 * convb[at, :].astype(F32))
            k = 1
            while k < ROWS:
                before = row >= k
                d = d + a * jnp.where(before, pltpu.roll(d, k, 0), 0.0)
                a = a * jnp.where(before, pltpu.roll(a, k, 0), 1.0)
                k *= 2
            d = d + a * carry[1]
            a = a * carry[0]
            cum_a[s, at, b] = a
            cum_b[s, at, b] = d
            return a[ROWS - 1 :], d[ROWS - 1 :]

        end = lax.fori_loop(
            0, rows // ROWS, scan, (jnp.ones((1, COLS), F32), jnp.zeros((1, COLS), F32)))
        my_ab[pl.ds(s, 1), b] = end[0]
        my_ab[pl.ds(seqs + s, 1), b] = end[1]

    for s in range(seqs):
        def chain_group(g, c, s=s):
            chain_step(g, s)
            return c

        for g0 in range(0, nb, 2):
            lax.fori_loop(g0, min(g0 + 2, nb), chain_group, 0)
            some_forwards(max(1, len(todo) // (2 * seqs)))

    def ab_copy(k):
        return pltpu.make_async_remote_copy(
            src_ref=my_ab, dst_ref=all_ab.at[k], send_sem=ab_s.at[k], recv_sem=ab_r.at[k],
            device_id={"sp": (sp + k) % n}, device_id_type=MESH)

    def pool_group(g):
        b = slice(g * COLS, (g + 1) * COLS)
        window = 2 ** (1 + g % 4)

        def diff(i, c):
            s, r = i // (rows // ROWS), pl.multiple_of((i % (rows // ROWS)) * ROWS, ROWS)
            v = pbuf[s, pl.ds(r, ROWS + HALO), b].astype(F32)
            total, k = v, 1
            while k < window:
                total = total + pltpu.roll(total, k, 0)
                k *= 2
            t = lax.broadcasted_iota(jnp.int32, (ROWS, COLS), 0) + (sp * rows + r + 1)
            count = jnp.minimum(t, window).astype(F32)
            convb_pool = total[HALO:] / count - v[HALO:]
            pooled[s, pl.ds(r, ROWS), b] = convb_pool.astype(BF16)
            return c

        lax.fori_loop(0, seqs * (rows // ROWS), diff, 0)
        for s in range(seqs):
            y = jnp.dot(pooled[s, :, b], pm[g], preferred_element_type=F32)
            pooled[s, :, b] = (y * pscale[:, b]).astype(BF16)

    pool_group(0)
    for k in range(1, n):
        @pl.when(sp + k < n)
        def _(k=k):
            ab_copy(k).start()

    for g in range(1, nb):
        pool_group(g)
        some_forwards(1)
    some_forwards(len(todo))

    ent[...] = start[...]
    for k in range(n - 1, 0, -1):
        @pl.when(sp >= k)
        def _(k=k):
            ab_copy(k).wait_recv()
            ent[...] = all_ab[k, :seqs, :] * ent[...] + all_ab[k, seqs : 2 * seqs, :]

    for s in range(seqs):
        def fix(i, c, s=s):
            at = pl.ds(pl.multiple_of(i * ROWS, ROWS), ROWS)
            rec[s, at, :] = (cum_a[s, at, :] * ent[s : s + 1, :] + cum_b[s, at, :]).astype(BF16)
            return c

        lax.fori_loop(0, rows // ROWS, fix, 0)

    dims = (((1,), (1,)), ((), ()))
    out_cols = sendbuf.shape[2]
    out_count = width // out_cols
    per_group = m * chain_exit.shape[0] // out_cols

    def out_lanes(j):
        return pl.ds(pl.multiple_of(j * out_cols, out_cols), out_cols)

    def partial(owner, j):
        at = pl.ds(pl.multiple_of(owner * half_rows, ROWS), half_rows)
        b = out_lanes(j)
        x = rec[:, at, :].reshape(seqs * half_rows, chans)
        y = pooled[:, at, :].reshape(seqs * half_rows, chans)
        return lax.dot_general(x, w2[b, :], dims, preferred_element_type=F32) + lax.dot_general(
            y, w3[b, :], dims, preferred_element_type=F32)

    def out_copy(j):
        return pltpu.make_async_remote_copy(
            src_ref=sendbuf.at[j], dst_ref=recvbuf.at[j], send_sem=out_s.at[j],
            recv_sem=out_r.at[j], device_id={"tp": 1 - tp}, device_id_type=MESH)

    def exit_step(j, c):
        sendbuf[j] = partial(1 - tp, j).astype(BF16)
        acc[j] = partial(tp, j)
        out_copy(j).start()
        return c

    def out_step(j, c):
        out_copy(j).wait_recv()
        total = (acc[j] + recvbuf[j].astype(F32)).astype(BF16)
        out[:, :, out_lanes(j)] = total.reshape(seqs, half_rows, out_cols)
        return c

    def group(p, step):
        j = ((sp + p) % n) * per_group
        lax.fori_loop(j, j + per_group, step, 0)

    before = None
    for p in [0] + order:
        for w in (2, 3):
            last_wait(w, p)
        group(p, exit_step)
        if before is not None:
            group(before, out_step)
        before = p
    group(before, out_step)

    def out_end(j, c):
        out_copy(j).wait_send()
        return c

    lax.fori_loop(0, out_count, out_end, 0)
    for copy in started:
        copy.wait_send()

    @pl.when(sp < n - 1)
    def _():
        halo(0, cbuf).wait_send()
        halo(1, pbuf).wait_send()

    for k in range(1, n):
        @pl.when(sp + k < n)
        def _(k=k):
            ab_copy(k).wait_send()


def per_device(n, m, *args):
    (tokens, norm_gain, chain_entry, pool_entry, conv_taps, recur_gate, input_gate, decay_log,
     decay_shift, start_state, pool_mix, pool_scale, chain_exit, pool_exit) = args
    seqs, half_rows, width = tokens.shape
    rows, chans = 2 * half_rows, chain_entry.shape[1]
    nb = chans // COLS
    assert pool_mix.shape[0] % 4 == 0 and pool_mix.shape[1] == COLS
    far = max(m // 2, 1)
    hbm, vmem = pl.BlockSpec(memory_space=pl.ANY), pl.BlockSpec(memory_space=pltpu.VMEM)
    dma = pltpu.SemaphoreType.DMA
    ab_rows = -(-2 * seqs // 8) * 8
    out_cols = min(COLS, m * chain_exit.shape[1])
    out_count = width // out_cols
    scratch = [pltpu.VMEM((width, chans), BF16)] * 4 + [
        pltpu.VMEM((seqs, half_rows, width), BF16),
        pltpu.VMEM((seqs, rows, width), BF16),
        pltpu.VMEM((seqs, HALO + rows, chans), BF16),
        pltpu.VMEM((seqs, HALO + rows, chans), BF16),
        pltpu.VMEM((seqs, rows, chans), F32),
        pltpu.VMEM(recur_gate.shape, BF16),
        pltpu.VMEM(input_gate.shape, BF16),
        pltpu.VMEM(pool_mix.shape, BF16),
        pltpu.VMEM((rows, COLS), BF16),
        pltpu.VMEM((rows, COLS), F32),
        pltpu.VMEM((rows, COLS), F32),
        pltpu.VMEM((seqs, rows, chans), F32),
        pltpu.VMEM((seqs, rows, chans), F32),
        pltpu.VMEM((seqs, rows, chans), BF16),
        pltpu.VMEM((seqs, rows, chans), BF16),
        pltpu.VMEM((ab_rows, chans), F32),
        pltpu.VMEM((n, ab_rows, chans), F32),
        pltpu.VMEM((seqs, chans), F32),
        pltpu.VMEM((out_count, seqs * half_rows, out_cols), F32),
        pltpu.VMEM((out_count, seqs * half_rows, out_cols), BF16),
        pltpu.VMEM((out_count, seqs * half_rows, out_cols), BF16),
        dma((4 * n,)), dma((4 * n,)), dma((8 * n * far,)), dma((8 * n * far,)),
        dma((4 * m,)), dma((4 * m,)), dma((4 * m * n,)), dma((4 * m * n,)),
        dma((9,)), dma((2,)), dma((2,)), dma((2,)), dma((n,)), dma((n,)),
        dma((out_count,)), dma((out_count,)),
    ]
    return pl.pallas_call(
        functools.partial(kernel, n, m),
        name="layer",
        out_shape=jax.ShapeDtypeStruct(tokens.shape, BF16),
        in_specs=[hbm, vmem, hbm, hbm, vmem, hbm, hbm, vmem, hbm, vmem, hbm, vmem, hbm, hbm],
        out_specs=vmem,
        scratch_shapes=scratch,
        compiler_params=pltpu.CompilerParams(
            collective_id=0, has_side_effects=True, vmem_limit_bytes=62 * 1024 * 1024),
    )(tokens, norm_gain[None], chain_entry, pool_entry, conv_taps, recur_gate, input_gate,
      decay_log[None], decay_shift, start_state, pool_mix, pool_scale[None],
      chain_exit.T, pool_exit.T)


def solution(mesh):
    in_specs = (
        P("fs", ("sp", "tp"), None),
        P(),
        P(("sp", "fs"), "tp"),
        P(("sp", "fs"), "tp"),
        P(None, "tp"),
        P("tp", None, None),
        P("tp", None, None),
        P("tp"),
        P("fs", "sp", "tp"),
        P("fs", "tp"),
        P("tp", None, None),
        P("tp"),
        P("tp", ("sp", "fs")),
        P("tp", ("sp", "fs")),
    )
    out_specs = P("fs", ("sp", "tp"), None)
    return jax.shard_map(
        functools.partial(per_device, mesh.shape["sp"], mesh.shape["fs"]),
        mesh=mesh, in_specs=in_specs, out_specs=out_specs, check_vma=False)
```

profile of v0, /device:TPU:23, one launch (start us, length us, event | category | flops | bytes accessed | tf_op | source)
XLA Modules:
  0.0 169.9 jit_solution(17370708330373236284)
XLA Ops:
  0.0 1.8 %copy.15 = bf16[1024,128]{0,1:T(8,128)(2,1)} copy(bf16[1024,128]{1,0:T(8,128)(2,1)} %param.26) | data formatting | bytes 524288 | tf_op args[12]
  1.8 1.8 %copy.16 = bf16[1024,128]{0,1:T(8,128)(2,1)} copy(bf16[1024,128]{1,0:T(8,128)(2,1)} %param.27) | data formatting | bytes 524288 | tf_op args[13]
  3.6 163.6 %layer.1 = bf16[2,192,2048]{2,1,0:T(8,128)(2,1)} custom-call(bf16[2,192,2048]{2,1,0:T(8,128)(2,1)} %tokens.1, f32[1,2048]{1,0:T(1,128)} %bitcast.7, bf16[128,1024]{1,0:T(8,128)(2,1)} %chain_entry.1, bf16[128,1024]{1,0:T(8,128)(2,1)} %pool_entry.1, bf16[4,1024]{1,0:T(4,128)(2,1)} %taps.1, bf16[4,256,256]{2,1,0:T(8,128)(2,1)} %rgate.1, ...), custom_call_target="tpu_custom_call" | custom-call | tf_op jit(solution)/shard_map/layer/pallas_call | solution.py:499
  167.2 2.7 %copy.18 = bf16[2,192,2048]{2,1,0:T(8,128)(2,1)} copy(bf16[2,192,2048]{2,1,0:T(8,128)(2,1)} %layer.1) | data formatting | bytes 3145728
where the time goes:
time: 170 us
  Pallas kernels  164 us (96%)
  local copies, waits for them, and re-layouts  6.31 us (4%)
    pallas_call x1, Pallas kernels, per_device(): pl.pallas_call(functools.partial(kernel, n, m), name='layer', out_shape=j...  164 us
    unnamed x3, local copies, waits for them, and re-layouts  6.31 us

commit v1 on v0

--- a/solution.py
+++ b/solution.py
@@ -13,6 +13,9 @@
 HALO = 16
 COLS = 256
 ROWS = 64
+ENTRY = (0, 1)
+EXIT = (2, 3)
+OWN, PEER = 0, 1
 F32 = jnp.float32
 BF16 = jnp.bfloat16
 
@@ -25,7 +28,571 @@
     return jnp.where(y < 0.5, y * poly, 1.0 - jnp.exp(x))
 
 
+def nearest(n):
+    order = [sorted(range(n), key=lambda z, s=s: (abs(z - s), (z - s) * (1 if 2 * s < n else -1)))
+             for s in range(n)]
+    return [sum(order[s][r] * n**s for s in range(n)) for r in range(n)]
+
+
 def kernel(
+    n, m,
+    tokens, gain, chain_entry, pool_entry, taps, rgate, igate, dlog, shift_hbm, start,
+    pmix, pscale, chain_exit, pool_exit,
+    out,
+    w0, w1, w2, w3, raw, normed, cacc, pacc, cbuf, pbuf, shift, wide, narrow, peer_shift,
+    my_start, peer_start, rg, ig, pm,
+    convb, zr, zi, cum_a, cum_b, rec, pooled, my_ab, all_ab, ent,
+    acc, core_send, core_recv, x_send, x_recv,
+    xs, xr, zs, zrv, ys, yr, loc, nsem_s, nsem_r, ssem_s, ssem_r, hsem_s, hsem_r, ab_s, ab_r,
+    core_s, core_r, out_s, out_r,
+):
+    sp, fs, tp = lax.axis_index("sp"), lax.axis_index("fs"), lax.axis_index("tp")
+    ny = m // 2
+    x, y = fs % 2, fs // 2
+    shards = (chain_entry, pool_entry, chain_exit, pool_exit)
+    bufs = (w0, w1, w2, w3)
+    seqs, half_rows, width = raw.shape
+    rows = 2 * half_rows
+    half = cbuf.shape[2]
+    nb = half // COLS
+    depth = chain_entry.shape[0]
+    out_cols = 2 * chain_exit.shape[1]
+    zdepth = m * depth
+
+    codes = nearest(n)
+
+    def digit(code):
+        value = sp * 0
+        for s in range(n):
+            value = value + code // n**s % n * jnp.where(sp == s, 1, 0)
+        return value
+
+    ranks = [digit(code) for code in codes]
+    x_peer = {"fs": y * 2 + 1 - x}
+    core_peer = {"tp": 1 - tp}
+
+    def y_peer(k):
+        return {"fs": ((y + k) % ny) * 2 + x}
+
+    barrier = pltpu.get_barrier_semaphore()
+    greet = [{"sp": (sp + k) % n} for k in range(1, n)] + [core_peer, x_peer]
+    greet += [y_peer(k) for k in range(1, ny)]
+    for device in greet:
+        pl.semaphore_signal(barrier, inc=1, device_id=device, device_id_type=MESH)
+
+    started = []
+
+    def launch(copy, cond=None):
+        if cond is None:
+            copy.start()
+        else:
+            pl.when(cond)(copy.start)
+        started.append((copy, cond))
+
+    def remote(src, dst, send, recv, device):
+        return pltpu.make_async_remote_copy(
+            src_ref=src, dst_ref=dst, send_sem=send, recv_sem=recv, device_id=device,
+            device_id_type=MESH)
+
+    def region(w, z, yy, xx):
+        b = z * m + yy * 2 + xx
+        if w in ENTRY:
+            return bufs[w].at[pl.ds(pl.multiple_of(b * depth, depth), depth)]
+        return bufs[w].at[b]
+
+    def shard(w, h):
+        at = pl.ds(pl.multiple_of(h * half, half), half)
+        return shards[w].at[:, at] if w in ENTRY else shards[w].at[at]
+
+    def cross(w):
+        return remote(shard(w, 1 - x), region(w, sp, y, x), xs.at[w], xr.at[w], x_peer)
+
+    def cross_wait(w):
+        ref = region(w, sp, y, 1 - x)
+        remote(ref, ref, xs.at[w], xr.at[w], x_peer).wait_recv()
+
+    def z_copy(w, z, xx, way, src=None):
+        ref = region(w, z, y, xx)
+        at = (w * n + z) * 2 + xx
+        return remote(ref if src is None else src, ref, zs.at[at * 2 + way], zrv.at[at],
+                      {"sp": (sp + (1, n - 1)[way]) % n})
+
+    def y_copy(w, z, xx, k, src=None):
+        ref = region(w, z, y, xx)
+        at = ((w * n + z) * 2 + xx) * ny + k
+        return remote(ref if src is None else src, ref, ys.at[at], yr.at[at], y_peer(k))
+
+    def y_wait(w, z, xx, k):
+        ref = region(w, z, (y + ny - k) % ny, xx)
+        at = ((w * n + z) * 2 + xx) * ny + k
+        remote(ref, ref, ys.at[at], yr.at[at], y_peer(k)).wait_recv()
+
+    def pass_on(w, r, xx, src=None):
+        z = ranks[r]
+        if n > 1:
+            launch(z_copy(w, z, xx, 0, src), (z <= sp) & (sp < n - 1))
+            launch(z_copy(w, z, xx, 1, src), (z >= sp) & (sp > 0))
+        for k in range(1, ny):
+            launch(y_copy(w, z, xx, k, src))
+
+    def forward(kinds, r):
+        for unit in (0, 1):
+            xx = x if unit == 0 else 1 - x
+            for w in kinds:
+                if r == 0 and unit == 0:
+                    pass_on(w, r, xx, shard(w, x))
+                    continue
+                if r == 0:
+                    cross_wait(w)
+                else:
+                    z_copy(w, ranks[r], xx, 0).wait_recv()
+                pass_on(w, r, xx)
+
+    def arrived(kinds, r, k):
+        if k:
+            for w in kinds:
+                for xx in (0, 1):
+                    y_wait(w, ranks[r], xx, k)
+
+    def lanes(c, base=0):
+        return pl.ds(pl.multiple_of(base + c * COLS, COLS), COLS)
+
+    mine_lanes = pl.ds(pl.multiple_of(x * half, half), half)
+    peer_lanes = pl.ds(pl.multiple_of((1 - x) * half, half), half)
+    heads = pl.ds(x * nb, nb)
+
+    local = [
+        pltpu.make_async_copy(tokens, raw, loc.at[0]),
+        pltpu.make_async_copy(shift_hbm.at[:, :, peer_lanes], wide, loc.at[1]),
+        pltpu.make_async_copy(shift_hbm.at[:, :, mine_lanes], shift, loc.at[2]),
+        pltpu.make_async_copy(rgate.at[heads], rg, loc.at[3]),
+        pltpu.make_async_copy(igate.at[heads], ig, loc.at[4]),
+        pltpu.make_async_copy(pmix.at[heads], pm, loc.at[5]),
+    ] + [pltpu.make_async_copy(shard(w, x), region(w, sp, y, x), loc.at[6 + w]) for w in range(4)]
+    for copy in local:
+        copy.start()
+    my_start[...] = jnp.zeros(my_start.shape, F32)
+    my_start[:seqs, :] = start[:, peer_lanes]
+
+    pl.semaphore_wait(barrier, len(greet))
+    for w in ENTRY:
+        launch(cross(w))
+    for w in ENTRY:
+        pass_on(w, 0, x, shard(w, x))
+
+    local[0].wait()
+
+    def half_of(s, owner):
+        return normed.at[s, pl.ds(pl.multiple_of(owner * half_rows, ROWS), half_rows)]
+
+    def norm_x(s):
+        return remote(half_of(s, tp), half_of(seqs + s, tp), nsem_s.at[s], nsem_r.at[s], x_peer)
+
+    def norm_core(s):
+        return remote(half_of(s, tp), half_of(s, tp), nsem_s.at[seqs + s], nsem_r.at[seqs + s],
+                      core_peer)
+
+    for s in range(seqs):
+        def norm_step(i, c, s=s):
+            r = pl.multiple_of(i * ROWS, ROWS)
+            v = raw[s, pl.ds(r, ROWS), :].astype(F32)
+            scale = lax.rsqrt(jnp.mean(v * v, axis=-1, keepdims=True) + NORM_EPSILON)
+            normed[s, pl.ds(pl.multiple_of(tp * half_rows + r, ROWS), ROWS), :] = (
+                v * scale * gain[...]).astype(BF16)
+            return c
+
+        lax.fori_loop(0, half_rows // ROWS, norm_step, 0)
+        launch(norm_x(s))
+        launch(norm_core(s))
+    for w in EXIT:
+        launch(cross(w))
+
+    local[1].wait()
+
+    def narrow_step(i, c):
+        s, r = i // (rows // ROWS), pl.multiple_of((i % (rows // ROWS)) * ROWS, ROWS)
+        narrow[s, pl.ds(r, ROWS), :] = wide[s, pl.ds(r, ROWS), :].astype(BF16)
+        return c
+
+    lax.fori_loop(0, seqs * (rows // ROWS), narrow_step, 0)
+    shift_copy = remote(narrow, peer_shift, ssem_s.at[0], ssem_r.at[0], x_peer)
+    start_copy = remote(my_start, peer_start, ssem_s.at[1], ssem_r.at[1], x_peer)
+    launch(start_copy)
+    launch(shift_copy)
+    for copy in local[2:]:
+        copy.wait()
+
+    for w in ENTRY:
+        cross_wait(w)
+        pass_on(w, 0, 1 - x)
+
+    def entry_part(s, r, last):
+        at = pl.ds(pl.multiple_of(ranks[r] * zdepth, zdepth), zdepth)
+
+        def step(j, c):
+            b = lanes(j)
+            v = normed[s, :, at]
+            for w, total, dst in ((w0, cacc, cbuf), (w1, pacc, pbuf)):
+                part = jnp.dot(v, w[at, b], preferred_element_type=F32)
+                if r:
+                    part = total[s, :, b] + part
+                if last:
+                    dst[s, HALO:, b] = part.astype(BF16)
+                else:
+                    total[s, :, b] = part
+            return c
+
+        lax.fori_loop(0, nb, step, 0)
+
+    def core_wait(s):
+        ref = half_of(s, 1 - tp)
+        remote(ref, ref, nsem_s.at[seqs + s], nsem_r.at[seqs + s], core_peer).wait_recv()
+
+    def relay(s):
+        ref = half_of(seqs + s, tp)
+        remote(ref, ref, nsem_s.at[s], nsem_r.at[s], x_peer).wait_recv()
+        at = 2 * seqs + s
+        launch(remote(ref, ref, nsem_s.at[at], nsem_r.at[at], core_peer))
+
+    def relay_wait(s):
+        ref = half_of(seqs + s, 1 - tp)
+        at = 2 * seqs + s
+        remote(ref, ref, nsem_s.at[at], nsem_r.at[at], core_peer).wait_recv()
+
+    own = range(seqs)
+    last = n - 1
+    for r in range(1, n):
+        forward(ENTRY, r)
+        if r == 1:
+            for s in own:
+                core_wait(s)
+        if r == last:
+            forward(EXIT, 0)
+        for k in range(1, ny):
+            arrived(ENTRY, r - 1, k)
+        for s in own:
+            entry_part(s, r - 1, False)
+    for s in own:
+        relay(s)
+        relay_wait(s)
+        for r in range(last):
+            entry_part(seqs + s, r, False)
+    if n == 1:
+        forward(EXIT, 0)
+        for s in own:
+            core_wait(s)
+    for k in range(1, ny):
+        arrived(ENTRY, last, k)
+
+    def halo(pair, i):
+        ref = (cbuf, pbuf)[i]
+        at = pl.ds(pair * seqs, seqs)
+        return remote(ref.at[at, pl.ds(rows, HALO)], ref.at[at, pl.ds(0, HALO)],
+                      hsem_s.at[pair * 2 + i], hsem_r.at[pair * 2 + i], {"sp": (sp + 1) % n})
+
+    for pair in (PEER, OWN):
+        for s in own:
+            entry_part(pair * seqs + s, last, True)
+        for i in (0, 1):
+            launch(halo(pair, i), sp < n - 1)
+    if n > 1:
+        forward(EXIT, 1)
+
+    def halo_wait(pair):
+        @pl.when(sp > 0)
+        def _():
+            halo(pair, 0).wait_recv()
+            halo(pair, 1).wait_recv()
+
+        @pl.when(sp == 0)
+        def _():
+            zero = jnp.zeros((seqs, HALO, half), BF16)
+            cbuf[pair * seqs : (pair + 1) * seqs, :HALO, :] = zero
+            pbuf[pair * seqs : (pair + 1) * seqs, :HALO, :] = zero
+
+    tap_count = taps.shape[0]
+    inverse_length = 1.0 / (rows * n)
+
+    def chain(pair, s0):
+        s = pair * seqs + s0
+
+        def group(g, carry):
+            b = lanes(g)
+            whole = lanes(g, x * half)
+            tap = taps[:, whole].astype(F32)
+
+            def conv(i, c):
+                r = pl.multiple_of(i * ROWS, ROWS)
+                v = cbuf[s, pl.ds(r, ROWS + HALO), b].astype(F32)
+                total = v * tap[tap_count - 1 : tap_count]
+                for j in range(tap_count - 1):
+                    total = total + pltpu.roll(v, tap_count - 1 - j, 0) * tap[j : j + 1]
+                convb[pl.ds(r, ROWS), :] = total[HALO:].astype(BF16)
+                return c
+
+            lax.fori_loop(0, rows // ROWS, conv, 0)
+            v = convb[...]
+            zr[...] = jnp.dot(v, rg[g], preferred_element_type=F32)
+            zi[...] = jnp.dot(v, ig[g], preferred_element_type=F32)
+            rate = -RECUR_SCALE * (jnp.exp(dlog[:, whole]) * inverse_length)
+            row = lax.broadcasted_iota(jnp.int32, (ROWS, COLS), 0)
+            source = peer_shift if pair == PEER else shift
+
+            def scan(i, ends):
+                r = pl.multiple_of(i * ROWS, ROWS)
+                at = pl.ds(r, ROWS)
+                log_decay = (jax.nn.sigmoid(zr[at, :]) * rate
+                             + source[s0, at, b].astype(F32))
+                a = jnp.exp(log_decay)
+                d = (jnp.sqrt(neg_expm1(2.0 * log_decay)) * jax.nn.sigmoid(zi[at, :])
+                     * convb[at, :].astype(F32))
+                k = 1
+                while k < ROWS:
+                    before = row >= k
+                    d = d + a * jnp.where(before, pltpu.roll(d, k, 0), 0.0)
+                    a = a * jnp.where(before, pltpu.roll(a, k, 0), 1.0)
+                    k *= 2
+                d = d + a * ends[1]
+                a = a * ends[0]
+                cum_a[s, at, b] = a
+                cum_b[s, at, b] = d
+                return a[ROWS - 1 :], d[ROWS - 1 :]
+
+            end = lax.fori_loop(
+                0, rows // ROWS, scan, (jnp.ones((1, COLS), F32), jnp.zeros((1, COLS), F32)))
+            my_ab[pair, pl.ds(s0, 1), b] = end[0]
+            my_ab[pair, pl.ds(seqs + s0, 1), b] = end[1]
+            return carry
+
+        lax.fori_loop(0, nb, group, 0)
+
+    def ab_copy(pair, k):
+        at = pair * n + k
+        return remote(my_ab.at[pair], all_ab.at[at], ab_s.at[at], ab_r.at[at],
+                      {"sp": (sp + k) % n})
+
+    def ab_send(pair):
+        for k in range(1, n):
+            launch(ab_copy(pair, k), sp + k < n)
+
+    def pool(pair):
+        def group(g, window):
+            b = lanes(g)
+
+            def diff(i, c):
+                s = pair * seqs + i // (rows // ROWS)
+                r = pl.multiple_of((i % (rows // ROWS)) * ROWS, ROWS)
+                v = pbuf[s, pl.ds(r, ROWS + HALO), b].astype(F32)
+                total, k = v, 1
+                while k < window:
+                    total = total + pltpu.roll(total, k, 0)
+                    k *= 2
+                t = lax.broadcasted_iota(jnp.int32, (ROWS, COLS), 0) + (sp * rows + r + 1)
+                count = jnp.minimum(t, window).astype(F32)
+                pooled[s, pl.ds(r, ROWS), b] = (total[HALO:] / count - v[HALO:]).astype(BF16)
+                return c
+
+            lax.fori_loop(0, seqs * (rows // ROWS), diff, 0)
+            for s0 in own:
+                s = pair * seqs + s0
+                p = jnp.dot(pooled[s, :, b], pm[g], preferred_element_type=F32)
+                pooled[s, :, b] = (p * pscale[:, lanes(g, x * half)]).astype(BF16)
+
+        for xx in (0, 1):
+            @pl.when(x == xx)
+            def _(xx=xx):
+                for g in range(nb):
+                    group(g, 2 ** (1 + (xx * nb + g) % 4))
+
+    def fix(pair):
+        if pair == OWN:
+            entry_state = start[:, mine_lanes]
+        else:
+            remote(my_start, peer_start, ssem_s.at[1], ssem_r.at[1], x_peer).wait_recv()
+            entry_state = peer_start[:seqs, :]
+        ent[...] = entry_state
+        for k in range(n - 1, 0, -1):
+            @pl.when(sp >= k)
+            def _(k=k):
+                ab_copy(pair, k).wait_recv()
+                at = pair * n + k
+                ent[...] = all_ab[at, :seqs, :] * ent[...] + all_ab[at, seqs : 2 * seqs, :]
+
+        for s0 in own:
+            s = pair * seqs + s0
+
+            def step(i, c, s=s, s0=s0):
+                at = pl.ds(pl.multiple_of(i * ROWS, ROWS), ROWS)
+                rec[s, at, :] = (
+                    cum_a[s, at, :] * ent[s0 : s0 + 1, :] + cum_b[s, at, :]).astype(BF16)
+                return c
+
+            lax.fori_loop(0, rows // ROWS, step, 0)
+
+    groups = sorted(((r, k) for r in range(n) for k in range(ny)),
+                    key=lambda rk: rk[0] + 1.5 * rk[1])
+
+    def partial(pair, owner, c):
+        r, k = groups[c]
+        b = ranks[r] * m + ((y + ny - k) % ny) * 2
+        at = pl.ds(pl.multiple_of(owner * half_rows, ROWS), half_rows)
+        which = slice(pair * seqs, (pair + 1) * seqs)
+        u = rec[which, at, :].reshape(seqs * half_rows, half)
+        v = pooled[which, at, :].reshape(seqs * half_rows, half)
+        return jnp.dot(
+            u, jnp.concatenate([w2[b], w2[b + 1]], axis=1), preferred_element_type=F32
+        ) + jnp.dot(v, jnp.concatenate([w3[b], w3[b + 1]], axis=1), preferred_element_type=F32)
+
+    count = len(groups)
+
+    def core_copy(pair, c):
+        at = pair * count + c
+        return remote(core_send.at[at], core_recv.at[at], core_s.at[at], core_r.at[at], core_peer)
+
+    def x_copy(c):
+        return remote(x_send.at[c], x_recv.at[c], out_s.at[c], out_r.at[c], x_peer)
+
+    def exit_dots(pair, c):
+        at = pair * count + c
+        core_send[at] = partial(pair, 1 - tp, c).astype(BF16)
+        launch(core_copy(pair, c))
+        acc[at] = partial(pair, tp, c)
+
+    def exit_send(c):
+        at = PEER * count + c
+        core_copy(PEER, c).wait_recv()
+        x_send[c] = (acc[at] + core_recv[at].astype(F32)).astype(BF16)
+        launch(x_copy(c))
+
+    def exit_out(c):
+        r, k = groups[c]
+        at = OWN * count + c
+        core_copy(OWN, c).wait_recv()
+        x_copy(c).wait_recv()
+        total = acc[at] + core_recv[at].astype(F32) + x_recv[c].astype(F32)
+        col = (ranks[r] * ny + (y + ny - k) % ny) * out_cols
+        out[:, :, pl.ds(pl.multiple_of(col, out_cols), out_cols)] = (
+            total.astype(BF16).reshape(seqs, half_rows, out_cols))
+
+    halo_wait(PEER)
+    remote(narrow, peer_shift, ssem_s.at[0], ssem_r.at[0], x_peer).wait_recv()
+    for s0 in own:
+        chain(PEER, s0)
+    ab_send(PEER)
+    if n > 2:
+        forward(EXIT, 2)
+    pool(PEER)
+    for r in range(3, n):
+        forward(EXIT, r)
+    fix(PEER)
+
+    done = []
+
+    def peer_out(upto):
+        for c in range(len(done), min(upto, count)):
+            arrived(EXIT, *groups[c])
+            exit_dots(PEER, c)
+            done.append(c)
+        for c in done:
+            if c not in sent:
+                exit_send(c)
+                sent.append(c)
+
+    sent = []
+    peer_out(2)
+    halo_wait(OWN)
+    for s0 in own:
+        chain(OWN, s0)
+        peer_out(3 + s0)
+    ab_send(OWN)
+    pool(OWN)
+    peer_out(len(done) + 1)
+    fix(OWN)
+    ready = 0
+    while len(done) < count:
+        peer_out(len(done) + 1)
+        while ready < len(done):
+            exit_dots(OWN, ready)
+            ready += 1
+    while ready < count:
+        exit_dots(OWN, ready)
+        ready += 1
+    for c in range(count):
+        exit_out(c)
+
+    for copy, cond in started:
+        if cond is None:
+            copy.wait_send()
+        else:
+            pl.when(cond)(copy.wait_send)
+
+
+def per_device(n, m, *args):
+    (tokens, norm_gain, chain_entry, pool_entry, conv_taps, recur_gate, input_gate, decay_log,
+     decay_shift, start_state, pool_mix, pool_scale, chain_exit, pool_exit) = args
+    seqs, half_rows, width = tokens.shape
+    rows, half = 2 * half_rows, chain_entry.shape[1] // 2
+    nb = half // COLS
+    ny = m // 2
+    assert pool_mix.shape[0] % 4 == 0 and pool_mix.shape[1] == COLS and m % 2 == 0
+    hbm, vmem = pl.BlockSpec(memory_space=pl.ANY), pl.BlockSpec(memory_space=pltpu.VMEM)
+    dma = pltpu.SemaphoreType.DMA
+    ab_rows = -(-2 * seqs // 8) * 8
+    out_cols = 2 * chain_exit.shape[1]
+    count = n * ny
+    tile = (seqs * half_rows, out_cols)
+    scratch = [pltpu.VMEM((width, half), BF16)] * 2 + [
+        pltpu.VMEM((n * m, half, chain_exit.shape[1]), BF16)] * 2 + [
+        pltpu.VMEM((seqs, half_rows, width), BF16),
+        pltpu.VMEM((2 * seqs, rows, width), BF16),
+        pltpu.VMEM((2 * seqs, rows, half), F32),
+        pltpu.VMEM((2 * seqs, rows, half), F32),
+        pltpu.VMEM((2 * seqs, HALO + rows, half), BF16),
+        pltpu.VMEM((2 * seqs, HALO + rows, half), BF16),
+        pltpu.VMEM((seqs, rows, half), F32),
+        pltpu.VMEM((seqs, rows, half), F32),
+        pltpu.VMEM((seqs, rows, half), BF16),
+        pltpu.VMEM((seqs, rows, half), BF16),
+        pltpu.VMEM((8, half), F32),
+        pltpu.VMEM((8, half), F32),
+        pltpu.VMEM((nb, COLS, COLS), BF16),
+        pltpu.VMEM((nb, COLS, COLS), BF16),
+        pltpu.VMEM((nb, COLS, COLS), BF16),
+        pltpu.VMEM((rows, COLS), BF16),
+        pltpu.VMEM((rows, COLS), F32),
+        pltpu.VMEM((rows, COLS), F32),
+        pltpu.VMEM((2 * seqs, rows, half), F32),
+        pltpu.VMEM((2 * seqs, rows, half), F32),
+        pltpu.VMEM((2 * seqs, rows, half), BF16),
+        pltpu.VMEM((2 * seqs, rows, half), BF16),
+        pltpu.VMEM((2, ab_rows, half), F32),
+        pltpu.VMEM((2 * n, ab_rows, half), F32),
+        pltpu.VMEM((seqs, half), F32),
+        pltpu.VMEM((2 * count, *tile), F32),
+        pltpu.VMEM((2 * count, *tile), BF16),
+        pltpu.VMEM((2 * count, *tile), BF16),
+        pltpu.VMEM((count, *tile), BF16),
+        pltpu.VMEM((count, *tile), BF16),
+        dma((4,)), dma((4,)), dma((16 * n,)), dma((8 * n,)), dma((8 * n * ny,)),
+        dma((8 * n * ny,)), dma((10,)), dma((3 * seqs,)), dma((3 * seqs,)), dma((2,)), dma((2,)),
+        dma((4,)), dma((4,)), dma((2 * n,)), dma((2 * n,)), dma((2 * count,)),
+        dma((2 * count,)), dma((count,)), dma((count,)),
+    ]
+    return pl.pallas_call(
+        functools.partial(kernel, n, m),
+        name="layer",
+        out_shape=jax.ShapeDtypeStruct(tokens.shape, BF16),
+        in_specs=[hbm, vmem, hbm, hbm, vmem, hbm, hbm, vmem, hbm, vmem, hbm, vmem, hbm, hbm],
+        out_specs=vmem,
+        scratch_shapes=scratch,
+        compiler_params=pltpu.CompilerParams(
+            collective_id=0, has_side_effects=True, vmem_limit_bytes=63 * 1024 * 1024),
+    )(tokens, norm_gain[None], chain_entry, pool_entry, conv_taps, recur_gate, input_gate,
+      decay_log[None], decay_shift, start_state, pool_mix, pool_scale[None],
+      chain_exit, pool_exit)
+
+
+def ring_kernel(
     n, m,
     tokens, gain, chain_entry, pool_entry, taps, rgate, igate, dlog, shift_hbm, start,
     pmix, pscale, chain_exit, pool_exit,
@@ -456,7 +1023,7 @@
             ab_copy(k).wait_send()
 
 
-def per_device(n, m, *args):
+def ring_device(n, m, *args):
     (tokens, norm_gain, chain_entry, pool_entry, conv_taps, recur_gate, input_gate, decay_log,
      decay_shift, start_state, pool_mix, pool_scale, chain_exit, pool_exit) = args
     seqs, half_rows, width = tokens.shape
@@ -497,7 +1064,7 @@
         dma((out_count,)), dma((out_count,)),
     ]
     return pl.pallas_call(
-        functools.partial(kernel, n, m),
+        functools.partial(ring_kernel, n, m),
         name="layer",
         out_shape=jax.ShapeDtypeStruct(tokens.shape, BF16),
         in_specs=[hbm, vmem, hbm, hbm, vmem, hbm, hbm, vmem, hbm, vmem, hbm, vmem, hbm, hbm],
@@ -528,6 +1095,11 @@
         P("tp", ("sp", "fs")),
     )
     out_specs = P("fs", ("sp", "tp"), None)
+    n, m = mesh.shape["sp"], mesh.shape["fs"]
+
+    def layer(*args):
+        wide = m % 2 == 0 and args[12].shape[1] % 128 == 0
+        return (per_device if wide else ring_device)(n, m, *args)
+
     return jax.shard_map(
-        functools.partial(per_device, mesh.shape["sp"], mesh.shape["fs"]),
-        mesh=mesh, in_specs=in_specs, out_specs=out_specs, check_vma=False)
+        layer, mesh=mesh, in_specs=in_specs, out_specs=out_specs, check_vma=False)

time: 170 us -> 144 us (0.85)
  the two profiles are of different devices: /device:TPU:23 before, /device:TPU:0 now
where the time goes in v1:
time: 144 us
  Pallas kernels  141 us (98%)
  local copies, waits for them, and re-layouts  2.73 us (2%)
    pallas_call x1, Pallas kernels, per_device(): pl.pallas_call(functools.partial(kernel, n, m), name='layer', out_shape=j...  141 us

profile of v1, /device:TPU:0, one launch (start us, length us, event | category | flops | bytes accessed | tf_op | source)
XLA Modules:
  0.0 144.1 jit_solution(6732786028160473493)
XLA Ops:
  0.0 141.3 %layer.1 = bf16[2,192,2048]{2,1,0:T(8,128)(2,1)} custom-call(bf16[2,192,2048]{2,1,0:T(8,128)(2,1)} %tokens.1, f32[1,2048]{1,0:T(1,128)} %bitcast.3, bf16[128,1024]{1,0:T(8,128)(2,1)} %chain_entry.1, bf16[128,1024]{1,0:T(8,128)(2,1)} %pool_entry.1, bf16[4,1024]{1,0:T(4,128)(2,1)} %taps.1, bf16[4,256,256]{2,1,0:T(8,128)(2,1)} %rgate.1, ...), custom_call_target="tpu_custom_call" | custom-call | tf_op jit(solution)/shard_map/layer/pallas_call | solution.py:581
  141.3 2.7 %copy.16 = bf16[2,192,2048]{2,1,0:T(8,128)(2,1)} copy(bf16[2,192,2048]{2,1,0:T(8,128)(2,1)} %layer.1) | data formatting | bytes 3145728

commit v2 on v1

--- a/solution.py
+++ b/solution.py
@@ -16,6 +16,8 @@
 ENTRY = (0, 1)
 EXIT = (2, 3)
 OWN, PEER = 0, 1
+TURN = 1
+PEER_SLOTS = 4
 F32 = jnp.float32
 BF16 = jnp.bfloat16
 
@@ -29,7 +31,7 @@
 
 
 def nearest(n):
-    order = [sorted(range(n), key=lambda z, s=s: (abs(z - s), (z - s) * (1 if 2 * s < n else -1)))
+    order = [sorted(range(n), key=lambda z, s=s: (abs(z - s), (z - s) * (-1 if 2 * s < n else 1)))
              for s in range(n)]
     return [sum(order[s][r] * n**s for s in range(n)) for r in range(n)]
 
@@ -39,25 +41,29 @@
     tokens, gain, chain_entry, pool_entry, taps, rgate, igate, dlog, shift_hbm, start,
     pmix, pscale, chain_exit, pool_exit,
     out,
-    w0, w1, w2, w3, raw, normed, cacc, pacc, cbuf, pbuf, shift, wide, narrow, peer_shift,
+    w0, w1, exits, raw, normed, cum_a, cum_b, cbuf, pbuf, shift, wide, narrow, peer_shift,
     my_start, peer_start, rg, ig, pm,
-    convb, zr, zi, cum_a, cum_b, rec, pooled, my_ab, all_ab, ent,
-    acc, core_send, core_recv, x_send, x_recv,
-    xs, xr, zs, zrv, ys, yr, loc, nsem_s, nsem_r, ssem_s, ssem_r, hsem_s, hsem_r, ab_s, ab_r,
-    core_s, core_r, out_s, out_r,
+    convb, zr, zi, mix, my_ab, all_ab, ent,
+    peer_acc, own_acc, core_send, core_recv, x_send, x_recv,
+    xs, xr, zs, zrv, zts, ztr, ys, yr, loc, nsem_s, nsem_r, ssem_s, ssem_r, hsem_s, hsem_r,
+    ab_s, ab_r, core_s, core_r, out_s, out_r,
 ):
+    scope = jax.named_scope
     sp, fs, tp = lax.axis_index("sp"), lax.axis_index("fs"), lax.axis_index("tp")
     ny = m // 2
     x, y = fs % 2, fs // 2
     shards = (chain_entry, pool_entry, chain_exit, pool_exit)
-    bufs = (w0, w1, w2, w3)
+    bufs = (w0, w1)
     seqs, half_rows, width = raw.shape
     rows = 2 * half_rows
     half = cbuf.shape[2]
+    rec, pooled = mix.at[:, :, pl.ds(0, half)], mix.at[:, :, pl.ds(half, half)]
     nb = half // COLS
     depth = chain_entry.shape[0]
-    out_cols = 2 * chain_exit.shape[1]
+    cols = chain_exit.shape[1]
     zdepth = m * depth
+    own = range(seqs)
+    last = n - 1
 
     codes = nearest(n)
 
@@ -68,11 +74,15 @@
         return value
 
     ranks = [digit(code) for code in codes]
+    units = (x, 1 - x)
     x_peer = {"fs": y * 2 + 1 - x}
     core_peer = {"tp": 1 - tp}
 
     def y_peer(k):
         return {"fs": ((y + k) % ny) * 2 + x}
+
+    def y_from(k):
+        return (y + ny - k) % ny
 
     barrier = pltpu.get_barrier_semaphore()
     greet = [{"sp": (sp + k) % n} for k in range(1, n)] + [core_peer, x_peer]
@@ -95,10 +105,11 @@
             device_id_type=MESH)
 
     def region(w, z, yy, xx):
-        b = z * m + yy * 2 + xx
         if w in ENTRY:
+            b = z * m + yy * 2 + xx
             return bufs[w].at[pl.ds(pl.multiple_of(b * depth, depth), depth)]
-        return bufs[w].at[b]
+        at = pl.ds((w - EXIT[0]) * half, half)
+        return exits.at[z * 2 + xx, at, pl.ds(pl.multiple_of(yy * cols, cols), cols)]
 
     def shard(w, h):
         at = pl.ds(pl.multiple_of(h * half, half), half)
@@ -110,12 +121,20 @@
     def cross_wait(w):
         ref = region(w, sp, y, 1 - x)
         remote(ref, ref, xs.at[w], xr.at[w], x_peer).wait_recv()
+
+    def z_peer(way):
+        return {"sp": (sp + (1, n - 1)[way]) % n}
 
     def z_copy(w, z, xx, way, src=None):
         ref = region(w, z, y, xx)
         at = (w * n + z) * 2 + xx
         return remote(ref if src is None else src, ref, zs.at[at * 2 + way], zrv.at[at],
-                      {"sp": (sp + (1, n - 1)[way]) % n})
+                      z_peer(way))
+
+    def z_turn(z, k, way):
+        ref = region(TURN, z, y_from(k), x)
+        at = z * ny + k
+        return remote(ref, ref, zts.at[at * 2 + way], ztr.at[at], z_peer(way))
 
     def y_copy(w, z, xx, k, src=None):
         ref = region(w, z, y, xx)
@@ -123,36 +142,98 @@
         return remote(ref if src is None else src, ref, ys.at[at], yr.at[at], y_peer(k))
 
     def y_wait(w, z, xx, k):
-        ref = region(w, z, (y + ny - k) % ny, xx)
+        ref = region(w, z, y_from(k), xx)
         at = ((w * n + z) * 2 + xx) * ny + k
         remote(ref, ref, ys.at[at], yr.at[at], y_peer(k)).wait_recv()
 
-    def pass_on(w, r, xx, src=None):
+    def source(w, unit):
+        return shard(w, x) if unit == 0 else None
+
+    def z_send(w, unit):
+        if n > 1:
+            launch(z_copy(w, sp, units[unit], 0, source(w, unit)), sp + 1 < n)
+            launch(z_copy(w, sp, units[unit], 1, source(w, unit)), sp > 0)
+
+    def exit_z_send(early):
+        toward = [sp + 2 == n, sp == 1]
+        for w in EXIT:
+            if n > 1:
+                for way, inside in ((0, sp + 1 < n), (1, sp > 0)):
+                    edge_link = toward[way] if n > 2 else sp < 0
+                    cond = inside & ((edge_link == False) if early else edge_link)
+                    launch(z_copy(w, sp, x, way, shard(w, x)), cond)
+
+    def turn_send():
+        for k in range(1, ny):
+            if n > 1:
+                launch(z_turn(sp, k, 0), sp + 1 < n)
+                launch(z_turn(sp, k, 1), sp > 0)
+
+    def y_send(w, unit):
+        for k in range(1, ny):
+            launch(y_copy(w, sp, units[unit], k, source(w, unit)))
+
+    def both(cond, other):
+        return other if cond is None else cond & other
+
+    def relay_on(z, make, cond):
+        if n > 2:
+            launch(make(0), both(cond, (z < sp) & (sp + 1 < n)))
+            launch(make(1), both(cond, (z > sp) & (sp > 0)))
+
+    def wait_if(make, cond):
+        if cond is None:
+            make().wait_recv()
+        else:
+            pl.when(cond)(lambda: make().wait_recv())
+
+    def forward(w, r, unit, cond=None):
+        z, xx = ranks[r], units[unit]
+        wait_if(lambda: z_copy(w, z, xx, 0), cond)
+        relay_on(z, lambda way: z_copy(w, z, xx, way), cond)
+        if (w, unit) != (TURN, 0):
+            for k in range(1, ny):
+                launch(y_copy(w, z, xx, k), cond)
+
+    def turn_forward(r, cond=None):
         z = ranks[r]
-        if n > 1:
-            launch(z_copy(w, z, xx, 0, src), (z <= sp) & (sp < n - 1))
-            launch(z_copy(w, z, xx, 1, src), (z >= sp) & (sp > 0))
         for k in range(1, ny):
-            launch(y_copy(w, z, xx, k, src))
-
-    def forward(kinds, r):
-        for unit in (0, 1):
-            xx = x if unit == 0 else 1 - x
-            for w in kinds:
-                if r == 0 and unit == 0:
-                    pass_on(w, r, xx, shard(w, x))
-                    continue
-                if r == 0:
+            wait_if(lambda k=k: z_turn(z, k, 0), cond)
+            relay_on(z, lambda way, k=k: z_turn(z, k, way), cond)
+
+    edge = (sp == 0) | (sp == n - 1)
+    inner = (sp > 0) & (sp < n - 1)
+
+    def entry_forward(r, cond=None, part=None):
+        todo = [(0, 0), (1, 0), (0, 1), (1, 1)]
+        todo = todo if part is None else (todo[:3], todo[3:])[part]
+        with scope(f"efwd#r={r}"):
+            for w, unit in todo:
+                forward(w, r, unit, cond)
+            if part != 0:
+                turn_forward(r, cond)
+
+    def entry_arrived(r):
+        for k in range(1, ny):
+            for w in ENTRY:
+                for unit in (0, 1):
+                    if (w, unit) != (TURN, 0):
+                        y_wait(w, ranks[r], units[unit], k)
+
+    def exit_arrived(r, unit):
+        for k in range(1, ny):
+            for w in EXIT:
+                y_wait(w, ranks[r], units[unit], k)
+
+    def exit_forward(r, unit, cond=None):
+        with scope(f"xfwd#r={r}#u={unit}"):
+            for w in EXIT:
+                if r:
+                    forward(w, r, unit, cond)
+                else:
                     cross_wait(w)
-                else:
-                    z_copy(w, ranks[r], xx, 0).wait_recv()
-                pass_on(w, r, xx)
-
-    def arrived(kinds, r, k):
-        if k:
-            for w in kinds:
-                for xx in (0, 1):
-                    y_wait(w, ranks[r], xx, k)
+                    z_send(w, unit)
+                    y_send(w, unit)
 
     def lanes(c, base=0):
         return pl.ds(pl.multiple_of(base + c * COLS, COLS), COLS)
@@ -174,11 +255,13 @@
     my_start[...] = jnp.zeros(my_start.shape, F32)
     my_start[:seqs, :] = start[:, peer_lanes]
 
-    pl.semaphore_wait(barrier, len(greet))
+    with scope("entry_barrier"):
+        pl.semaphore_wait(barrier, len(greet))
     for w in ENTRY:
         launch(cross(w))
     for w in ENTRY:
-        pass_on(w, 0, x, shard(w, x))
+        z_send(w, 0)
+        y_send(w, 0)
 
     local[0].wait()
 
@@ -192,7 +275,7 @@
         return remote(half_of(s, tp), half_of(s, tp), nsem_s.at[seqs + s], nsem_r.at[seqs + s],
                       core_peer)
 
-    for s in range(seqs):
+    for s in own:
         def norm_step(i, c, s=s):
             r = pl.multiple_of(i * ROWS, ROWS)
             v = raw[s, pl.ds(r, ROWS), :].astype(F32)
@@ -202,10 +285,6 @@
             return c
 
         lax.fori_loop(0, half_rows // ROWS, norm_step, 0)
-        launch(norm_x(s))
-        launch(norm_core(s))
-    for w in EXIT:
-        launch(cross(w))
 
     local[1].wait()
 
@@ -215,28 +294,40 @@
         return c
 
     lax.fori_loop(0, seqs * (rows // ROWS), narrow_step, 0)
-    shift_copy = remote(narrow, peer_shift, ssem_s.at[0], ssem_r.at[0], x_peer)
-    start_copy = remote(my_start, peer_start, ssem_s.at[1], ssem_r.at[1], x_peer)
-    launch(start_copy)
-    launch(shift_copy)
     for copy in local[2:]:
         copy.wait()
-
-    for w in ENTRY:
-        cross_wait(w)
-        pass_on(w, 0, 1 - x)
-
-    def entry_part(s, r, last):
+    start_copy = remote(my_start, peer_start, ssem_s.at[seqs], ssem_r.at[seqs], x_peer)
+
+    def shift_copy(s):
+        return remote(narrow.at[s], peer_shift.at[s], ssem_s.at[s], ssem_r.at[s], x_peer)
+
+    for s in own:
+        launch(norm_core(s))
+    with scope("cross_fwd"):
+        for w in ENTRY:
+            cross_wait(w)
+            z_send(w, 1)
+            y_send(w, 1)
+    launch(norm_x(0))
+    launch(start_copy)
+    for w in EXIT:
+        y_send(w, 0)
+    with scope("turn_fwd"):
+        for k in range(1, ny):
+            y_wait(TURN, sp, x, k)
+        turn_send()
+
+    def entry_part(s, r):
         at = pl.ds(pl.multiple_of(ranks[r] * zdepth, zdepth), zdepth)
 
         def step(j, c):
             b = lanes(j)
             v = normed[s, :, at]
-            for w, total, dst in ((w0, cacc, cbuf), (w1, pacc, pbuf)):
+            for w, total, dst in ((w0, cum_a, cbuf), (w1, cum_b, pbuf)):
                 part = jnp.dot(v, w[at, b], preferred_element_type=F32)
                 if r:
                     part = total[s, :, b] + part
-                if last:
+                if r == last:
                     dst[s, HALO:, b] = part.astype(BF16)
                 else:
                     total[s, :, b] = part
@@ -259,30 +350,60 @@
         at = 2 * seqs + s
         remote(ref, ref, nsem_s.at[at], nsem_r.at[at], core_peer).wait_recv()
 
-    own = range(seqs)
-    last = n - 1
-    for r in range(1, n):
-        forward(ENTRY, r)
+    def entry_parts(seqs_of, r):
+        with scope(f"edot#r={r}"):
+            for s in seqs_of:
+                entry_part(s, r)
+
+    def entry_ready(r):
+        with scope(f"earr#r={r}"):
+            entry_arrived(r)
+
+    peer = range(seqs, 2 * seqs)
+    for r in range(1, last):
+        entry_forward(r)
         if r == 1:
             for s in own:
                 core_wait(s)
-        if r == last:
-            forward(EXIT, 0)
-        for k in range(1, ny):
-            arrived(ENTRY, r - 1, k)
-        for s in own:
-            entry_part(s, r - 1, False)
-    for s in own:
-        relay(s)
-        relay_wait(s)
-        for r in range(last):
-            entry_part(seqs + s, r, False)
-    if n == 1:
-        forward(EXIT, 0)
+        entry_ready(r - 1)
+        entry_parts(own, r - 1)
+        if r == 1:
+            for s in own[1:]:
+                launch(norm_x(s))
+            exit_z_send(True)
+    if n > 1:
+        entry_forward(last, inner)
+    if n < 3:
         for s in own:
             core_wait(s)
-    for k in range(1, ny):
-        arrived(ENTRY, last, k)
+        for s in own[1:]:
+            launch(norm_x(s))
+        exit_z_send(True)
+    with scope("relay#s=0"):
+        relay(0)
+        relay_wait(0)
+    for r in range(last - 1):
+        entry_parts([seqs], r)
+    if n > 1:
+        entry_forward(last, edge, 0)
+        entry_ready(last - 1)
+        entry_parts(range(seqs + 1), last - 1)
+    with scope("relay#s=1"):
+        for s in own[1:]:
+            relay(s)
+    launch(shift_copy(0))
+    for w in EXIT:
+        launch(cross(w))
+    if n > 1:
+        entry_forward(last, edge, 1)
+    with scope("relay_wait#s=1"):
+        for s in own[1:]:
+            relay_wait(s)
+    for r in range(last):
+        entry_parts(range(seqs + 1, 2 * seqs), r)
+    exit_z_send(False)
+    with scope("earr_last"):
+        entry_arrived(last)
 
     def halo(pair, i):
         ref = (cbuf, pbuf)[i]
@@ -292,11 +413,15 @@
 
     for pair in (PEER, OWN):
         for s in own:
-            entry_part(pair * seqs + s, last, True)
+            entry_part(pair * seqs + s, last)
         for i in (0, 1):
             launch(halo(pair, i), sp < n - 1)
-    if n > 1:
-        forward(EXIT, 1)
+    for s in own[1:]:
+        launch(shift_copy(s))
+    for r in range(1, min(2, n)):
+        exit_forward(r, 0)
+    if n > 2:
+        exit_forward(2, 0, inner)
 
     def halo_wait(pair):
         @pl.when(sp > 0)
@@ -360,20 +485,18 @@
 
             end = lax.fori_loop(
                 0, rows // ROWS, scan, (jnp.ones((1, COLS), F32), jnp.zeros((1, COLS), F32)))
-            my_ab[pair, pl.ds(s0, 1), b] = end[0]
-            my_ab[pair, pl.ds(seqs + s0, 1), b] = end[1]
+            my_ab[s, pl.ds(0, 1), b] = end[0]
+            my_ab[s, pl.ds(1, 1), b] = end[1]
             return carry
 
-        lax.fori_loop(0, nb, group, 0)
-
-    def ab_copy(pair, k):
-        at = pair * n + k
-        return remote(my_ab.at[pair], all_ab.at[at], ab_s.at[at], ab_r.at[at],
-                      {"sp": (sp + k) % n})
-
-    def ab_send(pair):
+        with scope(f"chain#p={pair}#s={s0}"):
+            lax.fori_loop(0, nb, group, 0)
         for k in range(1, n):
-            launch(ab_copy(pair, k), sp + k < n)
+            launch(ab_copy(s, k), sp + k < n)
+
+    def ab_copy(s, k):
+        at = s * n + k
+        return remote(my_ab.at[s], all_ab.at[at], ab_s.at[at], ab_r.at[at], {"sp": (sp + k) % n})
 
     def pool(pair):
         def group(g, window):
@@ -398,133 +521,182 @@
                 p = jnp.dot(pooled[s, :, b], pm[g], preferred_element_type=F32)
                 pooled[s, :, b] = (p * pscale[:, lanes(g, x * half)]).astype(BF16)
 
-        for xx in (0, 1):
-            @pl.when(x == xx)
-            def _(xx=xx):
-                for g in range(nb):
-                    group(g, 2 ** (1 + (xx * nb + g) % 4))
-
-    def fix(pair):
-        if pair == OWN:
-            entry_state = start[:, mine_lanes]
-        else:
-            remote(my_start, peer_start, ssem_s.at[1], ssem_r.at[1], x_peer).wait_recv()
-            entry_state = peer_start[:seqs, :]
-        ent[...] = entry_state
-        for k in range(n - 1, 0, -1):
-            @pl.when(sp >= k)
-            def _(k=k):
-                ab_copy(pair, k).wait_recv()
-                at = pair * n + k
-                ent[...] = all_ab[at, :seqs, :] * ent[...] + all_ab[at, seqs : 2 * seqs, :]
-
-        for s0 in own:
-            s = pair * seqs + s0
-
-            def step(i, c, s=s, s0=s0):
+        with scope(f"pool#p={pair}"):
+            for xx in (0, 1):
+                @pl.when(x == xx)
+                def _(xx=xx):
+                    for g in range(nb):
+                        group(g, 2 ** (1 + (xx * nb + g) % 4))
+
+    def fix(pair, s0):
+        s = pair * seqs + s0
+        with scope(f"fix#p={pair}#s={s0}"):
+            if pair == OWN:
+                ent[s : s + 1, :] = start[s0 : s0 + 1, mine_lanes]
+            else:
+                ent[s : s + 1, :] = peer_start[s0 : s0 + 1, :]
+            for k in range(n - 1, 0, -1):
+                @pl.when(sp >= k)
+                def _(k=k):
+                    ab_copy(s, k).wait_recv()
+                    at = s * n + k
+                    ent[s : s + 1, :] = all_ab[at, 0:1, :] * ent[s : s + 1, :] + all_ab[at, 1:2, :]
+
+            def step(i, c):
                 at = pl.ds(pl.multiple_of(i * ROWS, ROWS), ROWS)
                 rec[s, at, :] = (
-                    cum_a[s, at, :] * ent[s0 : s0 + 1, :] + cum_b[s, at, :]).astype(BF16)
+                    cum_a[s, at, :] * ent[s : s + 1, :] + cum_b[s, at, :]).astype(BF16)
                 return c
 
             lax.fori_loop(0, rows // ROWS, step, 0)
 
-    groups = sorted(((r, k) for r in range(n) for k in range(ny)),
-                    key=lambda rk: rk[0] + 1.5 * rk[1])
-
-    def partial(pair, owner, c):
-        r, k = groups[c]
-        b = ranks[r] * m + ((y + ny - k) % ny) * 2
-        at = pl.ds(pl.multiple_of(owner * half_rows, ROWS), half_rows)
-        which = slice(pair * seqs, (pair + 1) * seqs)
-        u = rec[which, at, :].reshape(seqs * half_rows, half)
-        v = pooled[which, at, :].reshape(seqs * half_rows, half)
-        return jnp.dot(
-            u, jnp.concatenate([w2[b], w2[b + 1]], axis=1), preferred_element_type=F32
-        ) + jnp.dot(v, jnp.concatenate([w3[b], w3[b + 1]], axis=1), preferred_element_type=F32)
-
+    groups = [(unit, r) for unit in (0, 1) for r in range(n)]
     count = len(groups)
 
-    def core_copy(pair, c):
-        at = pair * count + c
+    def core_copy(at):
         return remote(core_send.at[at], core_recv.at[at], core_s.at[at], core_r.at[at], core_peer)
 
-    def x_copy(c):
-        return remote(x_send.at[c], x_recv.at[c], out_s.at[c], out_r.at[c], x_peer)
-
-    def exit_dots(pair, c):
-        at = pair * count + c
-        core_send[at] = partial(pair, 1 - tp, c).astype(BF16)
-        launch(core_copy(pair, c))
-        acc[at] = partial(pair, tp, c)
-
-    def exit_send(c):
-        at = PEER * count + c
-        core_copy(PEER, c).wait_recv()
-        x_send[c] = (acc[at] + core_recv[at].astype(F32)).astype(BF16)
-        launch(x_copy(c))
-
-    def exit_out(c):
-        r, k = groups[c]
-        at = OWN * count + c
-        core_copy(OWN, c).wait_recv()
-        x_copy(c).wait_recv()
-        total = acc[at] + core_recv[at].astype(F32) + x_recv[c].astype(F32)
-        col = (ranks[r] * ny + (y + ny - k) % ny) * out_cols
-        out[:, :, pl.ds(pl.multiple_of(col, out_cols), out_cols)] = (
-            total.astype(BF16).reshape(seqs, half_rows, out_cols))
-
-    halo_wait(PEER)
-    remote(narrow, peer_shift, ssem_s.at[0], ssem_r.at[0], x_peer).wait_recv()
+    def x_copy(s0, c):
+        at = c * seqs + s0
+        return remote(x_send.at[at], x_recv.at[at], out_s.at[at], out_r.at[at], x_peer)
+
+    def owner_rows(owner):
+        return pl.ds(pl.multiple_of(owner * half_rows, ROWS), half_rows)
+
+    def dots(pair, s0, c):
+        unit, r = groups[c]
+        s = pair * seqs + s0
+        b = ranks[r] * 2 + units[unit]
+        at = (pair * count + c) * seqs + s0
+        total = peer_acc.at[(c * seqs + s0) % PEER_SLOTS] if pair else own_acc.at[c * seqs + s0]
+        with scope(f"dots#p={pair}#s={s0}#c={c}"):
+            total[...] = jnp.dot(mix[s], exits[b], preferred_element_type=F32)
+            core_send[at] = total[owner_rows(1 - tp), :].astype(BF16)
+        launch(core_copy(at))
+
+    def peer_send(s0, c):
+        at = (PEER * count + c) * seqs + s0
+        with scope(f"send#s={s0}#c={c}"):
+            core_copy(at).wait_recv()
+            x_send[c * seqs + s0] = (
+                peer_acc[(c * seqs + s0) % PEER_SLOTS, owner_rows(tp), :]
+                + core_recv[at].astype(F32)).astype(BF16)
+        launch(x_copy(s0, c))
+
+    def own_out(s0, c):
+        unit, r = groups[c]
+        at = (OWN * count + c) * seqs + s0
+        other = groups.index((1 - unit, r))
+        with scope(f"out#s={s0}#c={c}"):
+            core_copy(at).wait_recv()
+            x_copy(s0, other).wait_recv()
+            total = (own_acc[c * seqs + s0, owner_rows(tp), :] + core_recv[at].astype(F32)
+                     + x_recv[other * seqs + s0].astype(F32)).astype(BF16)
+            for yy in range(ny):
+                col = (ranks[r] * m + yy * 2 + units[unit]) * cols
+                out[s0, :, pl.ds(pl.multiple_of(col, cols), cols)] = (
+                    total[:, yy * cols : (yy + 1) * cols])
+
+    waiting = []
+
+    def peer_step(s0, c, arrive=True):
+        if arrive:
+            with scope(f"xarr#c={c}"):
+                exit_arrived(groups[c][1], groups[c][0])
+        dots(PEER, s0, c)
+        flush()
+        waiting.append((s0, c))
+
+    def flush():
+        while waiting:
+            peer_send(*waiting.pop())
+
+    first = list(range(n))
+    second = list(range(n, 2 * n))
+    later = own[1:]
+
+    def forwards(r, unit, cond):
+        for rr in range(r, n if r == 3 else min(r + 1, n)):
+            exit_forward(rr, unit, cond)
+
+    with scope("halo_p"):
+        halo_wait(PEER)
+    forwards(3, 0, inner)
+    pool(PEER)
+    with scope("shift_wait#s=0"):
+        shift_copy(0).wait_recv()
+    chain(PEER, 0)
+    forwards(2, 0, edge)
+    exit_forward(0, 1)
+    with scope("start_wait"):
+        start_copy.wait_recv()
+    fix(PEER, 0)
+    for c in first[:2]:
+        peer_step(0, c)
+    flush()
+    forwards(3, 0, edge)
+    with scope("halo_o"):
+        halo_wait(OWN)
+    chain(OWN, 0)
+    for c in first[2:3]:
+        peer_step(0, c)
+    for s0 in later:
+        with scope(f"shift_wait#s={s0}"):
+            shift_copy(s0).wait_recv()
+        chain(PEER, s0)
+    forwards(1, 1, None)
+    forwards(2, 1, inner)
+    for c in first[3:]:
+        peer_step(0, c)
+    forwards(3, 1, inner)
+    for s0 in later:
+        fix(PEER, s0)
+        for c in first[:2]:
+            peer_step(s0, c, False)
+    forwards(2, 1, edge)
+    for s0 in later:
+        for c in first[2:]:
+            peer_step(s0, c, False)
     for s0 in own:
-        chain(PEER, s0)
-    ab_send(PEER)
-    if n > 2:
-        forward(EXIT, 2)
-    pool(PEER)
-    for r in range(3, n):
-        forward(EXIT, r)
-    fix(PEER)
-
-    done = []
-
-    def peer_out(upto):
-        for c in range(len(done), min(upto, count)):
-            arrived(EXIT, *groups[c])
-            exit_dots(PEER, c)
-            done.append(c)
-        for c in done:
-            if c not in sent:
-                exit_send(c)
-                sent.append(c)
-
-    sent = []
-    peer_out(2)
-    halo_wait(OWN)
+        peer_step(s0, second[0], s0 == 0)
+    flush()
+    for s0 in later:
+        chain(OWN, s0)
+    forwards(3, 1, edge)
+    for c in second[1:2]:
+        for s0 in own:
+            peer_step(s0, c, s0 == 0)
+    flush()
+    pool(OWN)
     for s0 in own:
-        chain(OWN, s0)
-        peer_out(3 + s0)
-    ab_send(OWN)
-    pool(OWN)
-    peer_out(len(done) + 1)
-    fix(OWN)
-    ready = 0
-    while len(done) < count:
-        peer_out(len(done) + 1)
-        while ready < len(done):
-            exit_dots(OWN, ready)
-            ready += 1
-    while ready < count:
-        exit_dots(OWN, ready)
-        ready += 1
-    for c in range(count):
-        exit_out(c)
-
-    for copy, cond in started:
-        if cond is None:
-            copy.wait_send()
-        else:
-            pl.when(cond)(copy.wait_send)
+        fix(OWN, s0)
+    for c in first:
+        for s0 in own:
+            dots(OWN, s0, c)
+    for c in second[2:3]:
+        for s0 in own:
+            peer_step(s0, c, s0 == 0)
+    flush()
+    for c in second[:2]:
+        for s0 in own:
+            dots(OWN, s0, c)
+    for c in second[3:]:
+        for s0 in own:
+            peer_step(s0, c, s0 == 0)
+    flush()
+    for c in second[2:]:
+        for s0 in own:
+            dots(OWN, s0, c)
+    for c in second + first:
+        for s0 in own:
+            own_out(s0, c)
+
+    with scope("drain"):
+        for copy, cond in started:
+            if cond is None:
+                copy.wait_send()
+            else:
+                pl.when(cond)(copy.wait_send)
 
 
 def per_device(n, m, *args):
@@ -534,15 +706,15 @@
     rows, half = 2 * half_rows, chain_entry.shape[1] // 2
     nb = half // COLS
     ny = m // 2
-    assert pool_mix.shape[0] % 4 == 0 and pool_mix.shape[1] == COLS and m % 2 == 0
+    assert pool_mix.shape[0] % 4 == 0 and pool_mix.shape[1] == COLS
     hbm, vmem = pl.BlockSpec(memory_space=pl.ANY), pl.BlockSpec(memory_space=pltpu.VMEM)
     dma = pltpu.SemaphoreType.DMA
-    ab_rows = -(-2 * seqs // 8) * 8
-    out_cols = 2 * chain_exit.shape[1]
-    count = n * ny
-    tile = (seqs * half_rows, out_cols)
+    cols = ny * chain_exit.shape[1]
+    count = 2 * n
+    total = (rows, cols)
+    tile = (half_rows, cols)
     scratch = [pltpu.VMEM((width, half), BF16)] * 2 + [
-        pltpu.VMEM((n * m, half, chain_exit.shape[1]), BF16)] * 2 + [
+        pltpu.VMEM((2 * n, 2 * half, cols), BF16),
         pltpu.VMEM((seqs, half_rows, width), BF16),
         pltpu.VMEM((2 * seqs, rows, width), BF16),
         pltpu.VMEM((2 * seqs, rows, half), F32),
@@ -561,22 +733,21 @@
         pltpu.VMEM((rows, COLS), BF16),
         pltpu.VMEM((rows, COLS), F32),
         pltpu.VMEM((rows, COLS), F32),
-        pltpu.VMEM((2 * seqs, rows, half), F32),
-        pltpu.VMEM((2 * seqs, rows, half), F32),
-        pltpu.VMEM((2 * seqs, rows, half), BF16),
-        pltpu.VMEM((2 * seqs, rows, half), BF16),
-        pltpu.VMEM((2, ab_rows, half), F32),
-        pltpu.VMEM((2 * n, ab_rows, half), F32),
-        pltpu.VMEM((seqs, half), F32),
-        pltpu.VMEM((2 * count, *tile), F32),
-        pltpu.VMEM((2 * count, *tile), BF16),
-        pltpu.VMEM((2 * count, *tile), BF16),
-        pltpu.VMEM((count, *tile), BF16),
-        pltpu.VMEM((count, *tile), BF16),
-        dma((4,)), dma((4,)), dma((16 * n,)), dma((8 * n,)), dma((8 * n * ny,)),
-        dma((8 * n * ny,)), dma((10,)), dma((3 * seqs,)), dma((3 * seqs,)), dma((2,)), dma((2,)),
-        dma((4,)), dma((4,)), dma((2 * n,)), dma((2 * n,)), dma((2 * count,)),
-        dma((2 * count,)), dma((count,)), dma((count,)),
+        pltpu.VMEM((2 * seqs, rows, 2 * half), BF16),
+        pltpu.VMEM((2 * seqs, 8, half), F32),
+        pltpu.VMEM((2 * seqs * n, 8, half), F32),
+        pltpu.VMEM((2 * seqs, half), F32),
+        pltpu.VMEM((PEER_SLOTS, *total), F32),
+        pltpu.VMEM((count * seqs, *total), F32),
+        pltpu.VMEM((2 * count * seqs, *tile), BF16),
+        pltpu.VMEM((2 * count * seqs, *tile), BF16),
+        pltpu.VMEM((count * seqs, *tile), BF16),
+        pltpu.VMEM((count * seqs, *tile), BF16),
+        dma((4,)), dma((4,)), dma((16 * n,)), dma((8 * n,)), dma((2 * n * ny,)), dma((n * ny,)),
+        dma((8 * n * ny,)), dma((8 * n * ny,)), dma((10,)), dma((3 * seqs,)), dma((3 * seqs,)),
+        dma((seqs + 1,)), dma((seqs + 1,)), dma((4,)), dma((4,)), dma((2 * seqs * n,)),
+        dma((2 * seqs * n,)), dma((2 * count * seqs,)), dma((2 * count * seqs,)),
+        dma((count * seqs,)), dma((count * seqs,)),
     ]
     return pl.pallas_call(
         functools.partial(kernel, n, m),

time: 144 us -> 127 us (0.88)
  Pallas kernels: 141 us -> 124 us
    pallas_call x1, Pallas kernels: 141 us -> 124 us  [per_device(): pl.pallas_call(functools.partial(kernel, n, m), name='layer', out_shape=j...]
where the time goes in v2:
time: 127 us; the launch traced here: 126 us
  Pallas kernels  124 us (98%)
  local copies, waits for them, and re-layouts  2.73 us (2%)
    pallas_call x1, Pallas kernels, per_device(): pl.pallas_call(functools.partial(kernel, n, m), name='layer', out_shape=j...  124 us
    unnamed x1, local copies, waits for them, and re-layouts  2.73 us

profile of v2, /device:TPU:0, one launch (start us, length us, event | category | flops | bytes accessed | tf_op | source)
XLA Modules:
  0.0 126.3 jit_solution(17695760300891826903)
XLA Ops:
  0.0 123.6 %layer.1 = bf16[2,192,2048]{2,1,0:T(8,128)(2,1)} custom-call(bf16[2,192,2048]{2,1,0:T(8,128)(2,1)} %tokens.1, f32[1,2048]{1,0:T(1,128)} %bitcast.3, bf16[128,1024]{1,0:T(8,128)(2,1)} %chain_entry.1, bf16[128,1024]{1,0:T(8,128)(2,1)} %pool_entry.1, bf16[4,1024]{1,0:T(4,128)(2,1)} %taps.1, bf16[4,256,256]{2,1,0:T(8,128)(2,1)} %rgate.1, ...), custom_call_target="tpu_custom_call" | custom-call | tf_op jit(solution)/shard_map/layer/pallas_call | solution.py:752
  123.6 2.7 %copy.16 = bf16[2,192,2048]{2,1,0:T(8,128)(2,1)} copy(bf16[2,192,2048]{2,1,0:T(8,128)(2,1)} %layer.1) | data formatting | bytes 3145728

commit v3 on v2

--- a/solution.py
+++ b/solution.py
@@ -17,7 +17,7 @@
 EXIT = (2, 3)
 OWN, PEER = 0, 1
 TURN = 1
-PEER_SLOTS = 4
+PEER_SLOTS = 2
 F32 = jnp.float32
 BF16 = jnp.bfloat16
 
@@ -125,25 +125,25 @@
     def z_peer(way):
         return {"sp": (sp + (1, n - 1)[way]) % n}
 
-    def z_copy(w, z, xx, way, src=None):
+    def z_copy(w, z, xx, way, src=None, home=False):
         ref = region(w, z, y, xx)
-        at = (w * n + z) * 2 + xx
-        return remote(ref if src is None else src, ref, zs.at[at * 2 + way], zrv.at[at],
-                      z_peer(way))
-
-    def z_turn(z, k, way):
+        at = (w * 2 + xx) * (n + 1)
+        return remote(ref if src is None else src, ref, zs.at[at + (n if home and way else z)],
+                      zrv.at[(w * 2 + xx) * n + z], z_peer(way))
+
+    def z_turn(z, k, way, home=False):
         ref = region(TURN, z, y_from(k), x)
-        at = z * ny + k
-        return remote(ref, ref, zts.at[at * 2 + way], ztr.at[at], z_peer(way))
+        at = (n if home and way else z) * (ny - 1) + k - 1
+        return remote(ref, ref, zts.at[at], ztr.at[z * (ny - 1) + k - 1], z_peer(way))
 
     def y_copy(w, z, xx, k, src=None):
         ref = region(w, z, y, xx)
-        at = ((w * n + z) * 2 + xx) * ny + k
+        at = ((w * n + z) * 2 + xx) * (ny - 1) + k - 1
         return remote(ref if src is None else src, ref, ys.at[at], yr.at[at], y_peer(k))
 
     def y_wait(w, z, xx, k):
         ref = region(w, z, y_from(k), xx)
-        at = ((w * n + z) * 2 + xx) * ny + k
+        at = ((w * n + z) * 2 + xx) * (ny - 1) + k - 1
         remote(ref, ref, ys.at[at], yr.at[at], y_peer(k)).wait_recv()
 
     def source(w, unit):
@@ -151,23 +151,22 @@
 
     def z_send(w, unit):
         if n > 1:
-            launch(z_copy(w, sp, units[unit], 0, source(w, unit)), sp + 1 < n)
-            launch(z_copy(w, sp, units[unit], 1, source(w, unit)), sp > 0)
-
-    def exit_z_send(early):
-        toward = [sp + 2 == n, sp == 1]
+            launch(z_copy(w, sp, units[unit], 0, source(w, unit), True), sp + 1 < n)
+            launch(z_copy(w, sp, units[unit], 1, source(w, unit), True), sp > 0)
+
+    def exit_z_send(unit, to_end):
+        ends = (sp + 2 == n, sp == 1) if n > 2 else (sp < 0, sp < 0)
         for w in EXIT:
             if n > 1:
                 for way, inside in ((0, sp + 1 < n), (1, sp > 0)):
-                    edge_link = toward[way] if n > 2 else sp < 0
-                    cond = inside & ((edge_link == False) if early else edge_link)
-                    launch(z_copy(w, sp, x, way, shard(w, x)), cond)
+                    end = ends[way] if to_end else jnp.logical_not(ends[way])
+                    launch(z_copy(w, sp, units[unit], way, source(w, unit), True), inside & end)
 
     def turn_send():
         for k in range(1, ny):
             if n > 1:
-                launch(z_turn(sp, k, 0), sp + 1 < n)
-                launch(z_turn(sp, k, 1), sp > 0)
+                launch(z_turn(sp, k, 0, True), sp + 1 < n)
+                launch(z_turn(sp, k, 1, True), sp > 0)
 
     def y_send(w, unit):
         for k in range(1, ny):
@@ -232,8 +231,13 @@
                     forward(w, r, unit, cond)
                 else:
                     cross_wait(w)
-                    z_send(w, unit)
                     y_send(w, unit)
+            if r == 0:
+                exit_z_send(unit, False)
+
+    def forwards(r, unit, cond):
+        for rr in range(r, n if r == 3 else min(r + 1, n)):
+            exit_forward(rr, unit, cond)
 
     def lanes(c, base=0):
         return pl.ds(pl.multiple_of(base + c * COLS, COLS), COLS)
@@ -308,7 +312,8 @@
             cross_wait(w)
             z_send(w, 1)
             y_send(w, 1)
-    launch(norm_x(0))
+            if w == ENTRY[0]:
+                launch(norm_x(0))
     launch(start_copy)
     for w in EXIT:
         y_send(w, 0)
@@ -368,17 +373,21 @@
         entry_ready(r - 1)
         entry_parts(own, r - 1)
         if r == 1:
+            for w in EXIT:
+                launch(cross(w))
             for s in own[1:]:
                 launch(norm_x(s))
-            exit_z_send(True)
+            exit_z_send(0, False)
     if n > 1:
         entry_forward(last, inner)
     if n < 3:
         for s in own:
             core_wait(s)
+        for w in EXIT:
+            launch(cross(w))
         for s in own[1:]:
             launch(norm_x(s))
-        exit_z_send(True)
+        exit_z_send(0, False)
     with scope("relay#s=0"):
         relay(0)
         relay_wait(0)
@@ -388,20 +397,21 @@
         entry_forward(last, edge, 0)
         entry_ready(last - 1)
         entry_parts(range(seqs + 1), last - 1)
+    exit_z_send(0, True)
+    forwards(1, 0, inner)
+    forwards(2, 0, inner)
+    if n > 1:
+        entry_forward(last, edge, 1)
+    exit_forward(0, 1)
     with scope("relay#s=1"):
         for s in own[1:]:
             relay(s)
     launch(shift_copy(0))
-    for w in EXIT:
-        launch(cross(w))
-    if n > 1:
-        entry_forward(last, edge, 1)
     with scope("relay_wait#s=1"):
         for s in own[1:]:
             relay_wait(s)
     for r in range(last):
         entry_parts(range(seqs + 1, 2 * seqs), r)
-    exit_z_send(False)
     with scope("earr_last"):
         entry_arrived(last)
 
@@ -418,10 +428,8 @@
             launch(halo(pair, i), sp < n - 1)
     for s in own[1:]:
         launch(shift_copy(s))
-    for r in range(1, min(2, n)):
-        exit_forward(r, 0)
-    if n > 2:
-        exit_forward(2, 0, inner)
+    forwards(1, 0, edge)
+    forwards(3, 0, inner)
 
     def halo_wait(pair):
         @pl.when(sp > 0)
@@ -495,7 +503,7 @@
             launch(ab_copy(s, k), sp + k < n)
 
     def ab_copy(s, k):
-        at = s * n + k
+        at = s * (n - 1) + k - 1
         return remote(my_ab.at[s], all_ab.at[at], ab_s.at[at], ab_r.at[at], {"sp": (sp + k) % n})
 
     def pool(pair):
@@ -539,7 +547,7 @@
                 @pl.when(sp >= k)
                 def _(k=k):
                     ab_copy(s, k).wait_recv()
-                    at = s * n + k
+                    at = s * (n - 1) + k - 1
                     ent[s : s + 1, :] = all_ab[at, 0:1, :] * ent[s : s + 1, :] + all_ab[at, 1:2, :]
 
             def step(i, c):
@@ -553,143 +561,148 @@
     groups = [(unit, r) for unit in (0, 1) for r in range(n)]
     count = len(groups)
 
-    def core_copy(at):
-        return remote(core_send.at[at], core_recv.at[at], core_s.at[at], core_r.at[at], core_peer)
-
-    def x_copy(s0, c):
-        at = c * seqs + s0
-        return remote(x_send.at[at], x_recv.at[at], out_s.at[at], out_r.at[at], x_peer)
+    def core_copy(pair, c, which):
+        at = pair * count + c
+        sem = c * seqs + which.start if pair else count * seqs + c
+        return remote(core_send.at[at, which], core_recv.at[at, which], core_s.at[sem],
+                      core_r.at[sem], core_peer)
+
+    def x_copy(c, which):
+        sem = c * seqs + which.start
+        return remote(x_send.at[c, which], x_recv.at[c, which], out_s.at[sem], out_r.at[sem],
+                      x_peer)
 
     def owner_rows(owner):
         return pl.ds(pl.multiple_of(owner * half_rows, ROWS), half_rows)
 
-    def dots(pair, s0, c):
+    def slot(which, c):
+        return slots.setdefault((c, which.start), len(slots) % PEER_SLOTS)
+
+    slots = {}
+
+    def dots(pair, which, c):
         unit, r = groups[c]
-        s = pair * seqs + s0
+        size = which.size
         b = ranks[r] * 2 + units[unit]
-        at = (pair * count + c) * seqs + s0
-        total = peer_acc.at[(c * seqs + s0) % PEER_SLOTS] if pair else own_acc.at[c * seqs + s0]
-        with scope(f"dots#p={pair}#s={s0}#c={c}"):
-            total[...] = jnp.dot(mix[s], exits[b], preferred_element_type=F32)
-            core_send[at] = total[owner_rows(1 - tp), :].astype(BF16)
-        launch(core_copy(at))
-
-    def peer_send(s0, c):
-        at = (PEER * count + c) * seqs + s0
-        with scope(f"send#s={s0}#c={c}"):
-            core_copy(at).wait_recv()
-            x_send[c * seqs + s0] = (
-                peer_acc[(c * seqs + s0) % PEER_SLOTS, owner_rows(tp), :]
-                + core_recv[at].astype(F32)).astype(BF16)
-        launch(x_copy(s0, c))
-
-    def own_out(s0, c):
+        total = peer_acc.at[slot(which, c), which] if pair else own_acc.at[c, which]
+        with scope(f"dots#p={pair}#s={which.start}#c={c}"):
+            def part(owner):
+                v = mix[pl.ds(pair * seqs + which.start, size), owner_rows(owner), :]
+                v = v.reshape(size * half_rows, 2 * half)
+                return jnp.dot(v, exits[b], preferred_element_type=F32).reshape(total.shape)
+
+            core_send[pair * count + c, which] = part(1 - tp).astype(BF16)
+            total[...] = part(tp)
+        launch(core_copy(pair, c, which))
+
+    def peer_send(which, c):
+        with scope(f"send#s={which.start}#c={c}"):
+            core_copy(PEER, c, which).wait_recv()
+            x_send[c, which] = (
+                peer_acc[slot(which, c), which]
+                + core_recv[PEER * count + c, which].astype(F32)).astype(BF16)
+        launch(x_copy(c, which))
+        sent[c].append(which)
+
+    sent = [[] for _ in groups]
+
+    def own_out(c):
         unit, r = groups[c]
-        at = (OWN * count + c) * seqs + s0
         other = groups.index((1 - unit, r))
-        with scope(f"out#s={s0}#c={c}"):
-            core_copy(at).wait_recv()
-            x_copy(s0, other).wait_recv()
-            total = (own_acc[c * seqs + s0, owner_rows(tp), :] + core_recv[at].astype(F32)
-                     + x_recv[other * seqs + s0].astype(F32)).astype(BF16)
+        with scope(f"out#c={c}"):
+            core_copy(OWN, c, every).wait_recv()
+            for which in sent[other]:
+                x_copy(other, which).wait_recv()
+            total = (own_acc[c] + core_recv[OWN * count + c].astype(F32)
+                     + x_recv[other].astype(F32)).astype(BF16)
             for yy in range(ny):
                 col = (ranks[r] * m + yy * 2 + units[unit]) * cols
-                out[s0, :, pl.ds(pl.multiple_of(col, cols), cols)] = (
-                    total[:, yy * cols : (yy + 1) * cols])
-
+                out[:, :, pl.ds(pl.multiple_of(col, cols), cols)] = (
+                    total[:, :, yy * cols : (yy + 1) * cols])
+
+    every = pl.ds(0, seqs)
     waiting = []
-
-    def peer_step(s0, c, arrive=True):
-        if arrive:
+    seen = set()
+
+    def peer_step(which, c):
+        if c not in seen:
+            seen.add(c)
             with scope(f"xarr#c={c}"):
                 exit_arrived(groups[c][1], groups[c][0])
-        dots(PEER, s0, c)
+        dots(PEER, which, c)
         flush()
-        waiting.append((s0, c))
+        waiting.append((which, c))
 
     def flush():
         while waiting:
             peer_send(*waiting.pop())
 
-    first = list(range(n))
-    second = list(range(n, 2 * n))
+    own_units = list(range(n))
+    peer_units = list(range(n, 2 * n))
     later = own[1:]
-
-    def forwards(r, unit, cond):
-        for rr in range(r, n if r == 3 else min(r + 1, n)):
-            exit_forward(rr, unit, cond)
 
     with scope("halo_p"):
         halo_wait(PEER)
-    forwards(3, 0, inner)
     pool(PEER)
+    forwards(2, 0, edge)
     with scope("shift_wait#s=0"):
         shift_copy(0).wait_recv()
     chain(PEER, 0)
-    forwards(2, 0, edge)
-    exit_forward(0, 1)
+    exit_z_send(1, True)
+    forwards(1, 1, inner)
+    forwards(2, 1, inner)
     with scope("start_wait"):
         start_copy.wait_recv()
     fix(PEER, 0)
-    for c in first[:2]:
-        peer_step(0, c)
+    lead = own_units[:2] + peer_units[:1] + own_units[2:3]
+    for c in lead:
+        peer_step(pl.ds(0, 1), c)
     flush()
     forwards(3, 0, edge)
-    with scope("halo_o"):
-        halo_wait(OWN)
-    chain(OWN, 0)
-    for c in first[2:3]:
-        peer_step(0, c)
     for s0 in later:
         with scope(f"shift_wait#s={s0}"):
             shift_copy(s0).wait_recv()
         chain(PEER, s0)
-    forwards(1, 1, None)
-    forwards(2, 1, inner)
-    for c in first[3:]:
-        peer_step(0, c)
     forwards(3, 1, inner)
+    forwards(1, 1, edge)
+    with scope("halo_o"):
+        halo_wait(OWN)
+    pool(OWN)
+    tail = own_units[3:]
+    for c in tail:
+        peer_step(pl.ds(0, 1), c)
     for s0 in later:
         fix(PEER, s0)
-        for c in first[:2]:
-            peer_step(s0, c, False)
+        for c in lead + tail:
+            peer_step(pl.ds(s0, 1), c)
     forwards(2, 1, edge)
-    for s0 in later:
-        for c in first[2:]:
-            peer_step(s0, c, False)
-    for s0 in own:
-        peer_step(s0, second[0], s0 == 0)
+    flush()
+    chain(OWN, 0)
+    for c in peer_units[1:2]:
+        peer_step(every, c)
+    forwards(3, 1, edge)
+    fix(OWN, 0)
     flush()
     for s0 in later:
         chain(OWN, s0)
-    forwards(3, 1, edge)
-    for c in second[1:2]:
-        for s0 in own:
-            peer_step(s0, c, s0 == 0)
+    for c in peer_units[2:3]:
+        peer_step(every, c)
+    for s0 in later:
+        fix(OWN, s0)
+    for c in lead[:2]:
+        dots(OWN, every, c)
     flush()
-    pool(OWN)
-    for s0 in own:
-        fix(OWN, s0)
-    for c in first:
-        for s0 in own:
-            dots(OWN, s0, c)
-    for c in second[2:3]:
-        for s0 in own:
-            peer_step(s0, c, s0 == 0)
+    for c in peer_units[3:]:
+        peer_step(every, c)
+    for c in lead[2:4]:
+        dots(OWN, every, c)
     flush()
-    for c in second[:2]:
-        for s0 in own:
-            dots(OWN, s0, c)
-    for c in second[3:]:
-        for s0 in own:
-            peer_step(s0, c, s0 == 0)
-    flush()
-    for c in second[2:]:
-        for s0 in own:
-            dots(OWN, s0, c)
-    for c in second + first:
-        for s0 in own:
-            own_out(s0, c)
+    for c in lead[4:] + tail:
+        dots(OWN, every, c)
+    for c in peer_units[1:]:
+        dots(OWN, every, c)
+    for c in peer_units + own_units:
+        own_out(c)
 
     with scope("drain"):
         for copy, cond in started:
@@ -711,8 +724,8 @@
     dma = pltpu.SemaphoreType.DMA
     cols = ny * chain_exit.shape[1]
     count = 2 * n
-    total = (rows, cols)
-    tile = (half_rows, cols)
+    hops = ny - 1
+    tile = (seqs, half_rows, cols)
     scratch = [pltpu.VMEM((width, half), BF16)] * 2 + [
         pltpu.VMEM((2 * n, 2 * half, cols), BF16),
         pltpu.VMEM((seqs, half_rows, width), BF16),
@@ -735,29 +748,30 @@
         pltpu.VMEM((rows, COLS), F32),
         pltpu.VMEM((2 * seqs, rows, 2 * half), BF16),
         pltpu.VMEM((2 * seqs, 8, half), F32),
-        pltpu.VMEM((2 * seqs * n, 8, half), F32),
+        pltpu.VMEM((2 * seqs * (n - 1), 8, half), F32),
         pltpu.VMEM((2 * seqs, half), F32),
-        pltpu.VMEM((PEER_SLOTS, *total), F32),
-        pltpu.VMEM((count * seqs, *total), F32),
-        pltpu.VMEM((2 * count * seqs, *tile), BF16),
-        pltpu.VMEM((2 * count * seqs, *tile), BF16),
-        pltpu.VMEM((count * seqs, *tile), BF16),
-        pltpu.VMEM((count * seqs, *tile), BF16),
-        dma((4,)), dma((4,)), dma((16 * n,)), dma((8 * n,)), dma((2 * n * ny,)), dma((n * ny,)),
-        dma((8 * n * ny,)), dma((8 * n * ny,)), dma((10,)), dma((3 * seqs,)), dma((3 * seqs,)),
-        dma((seqs + 1,)), dma((seqs + 1,)), dma((4,)), dma((4,)), dma((2 * seqs * n,)),
-        dma((2 * seqs * n,)), dma((2 * count * seqs,)), dma((2 * count * seqs,)),
-        dma((count * seqs,)), dma((count * seqs,)),
+        pltpu.VMEM((PEER_SLOTS, *tile), F32),
+        pltpu.VMEM((count, *tile), F32),
+        pltpu.VMEM((2 * count, *tile), BF16),
+        pltpu.VMEM((2 * count, *tile), BF16),
+        pltpu.VMEM((count, *tile), BF16),
+        pltpu.VMEM((count, *tile), BF16),
+        dma((4,)), dma((4,)), dma((8 * (n + 1),)), dma((8 * n,)), dma(((n + 1) * hops,)),
+        dma((n * hops,)), dma((8 * n * hops,)), dma((8 * n * hops,)), dma((10,)),
+        dma((3 * seqs,)), dma((3 * seqs,)), dma((seqs + 1,)), dma((seqs + 1,)), dma((4,)),
+        dma((4,)), dma((2 * seqs * (n - 1),)), dma((2 * seqs * (n - 1),)),
+        dma((count * (seqs + 1),)), dma((count * (seqs + 1),)), dma((count * seqs,)),
+        dma((count * seqs,)),
     ]
     return pl.pallas_call(
         functools.partial(kernel, n, m),
         name="layer",
-        out_shape=jax.ShapeDtypeStruct(tokens.shape, BF16),
+        out_shape=pltpu.VMEM(tokens.shape, BF16),
         in_specs=[hbm, vmem, hbm, hbm, vmem, hbm, hbm, vmem, hbm, vmem, hbm, vmem, hbm, hbm],
         out_specs=vmem,
         scratch_shapes=scratch,
         compiler_params=pltpu.CompilerParams(
-            collective_id=0, has_side_effects=True, vmem_limit_bytes=63 * 1024 * 1024),
+            collective_id=0, has_side_effects=True, vmem_limit_bytes=60 * 1024 * 1024),
     )(tokens, norm_gain[None], chain_entry, pool_entry, conv_taps, recur_gate, input_gate,
       decay_log[None], decay_shift, start_state, pool_mix, pool_scale[None],
       chain_exit, pool_exit)
@@ -1269,7 +1283,7 @@
     n, m = mesh.shape["sp"], mesh.shape["fs"]
 
     def layer(*args):
-        wide = m % 2 == 0 and args[12].shape[1] % 128 == 0
+        wide = n > 1 and m > 2 and m % 2 == 0 and args[12].shape[1] % 128 == 0
         return (per_device if wide else ring_device)(n, m, *args)
 
     return jax.shard_map(

time: 127 us -> 115 us (0.906)
  Pallas kernels: 124 us -> 113 us
  local copies, waits for them, and re-layouts: 2.73 us -> 1.15 us
    pallas_call x1, Pallas kernels: 124 us -> 113 us  [per_device(): pl.pallas_call(functools.partial(kernel, n, m), name='layer', out_shape=p...]
    unnamed x1, local copies, waits for them, and re-layouts: 2.73 us -> 1.15 us
where the time goes in v3:
time: 115 us
  Pallas kernels  113 us (98%)
    pallas_call x1, Pallas kernels, per_device(): pl.pallas_call(functools.partial(kernel, n, m), name='layer', out_shape=p...  113 us

profile of v3, /device:TPU:0, one launch (start us, length us, event | category | flops | bytes accessed | tf_op | source)
XLA Modules:
  0.0 114.6 jit_solution(6116661451658255134)
XLA Ops:
  0.0 113.5 %layer.1 = bf16[2,192,2048]{2,1,0:T(8,128)(2,1)S(1)} custom-call(bf16[2,192,2048]{2,1,0:T(8,128)(2,1)} %tokens.1, f32[1,2048]{1,0:T(1,128)} %bitcast.3, bf16[128,1024]{1,0:T(8,128)(2,1)} %chain_entry.1, bf16[128,1024]{1,0:T(8,128)(2,1)} %pool_entry.1, bf16[4,1024]{1,0:T(4,128)(2,1)} %taps.1, bf16[4,256,256]{2,1,0:T(8,128)(2,1)} %rgate.1, ...), custom_call_target="tpu_custom_call" | custom-call | tf_op jit(solution)/shard_map/layer/pallas_call | solution.py:766
  113.5 1.1 copy.16

commit v4 on v3

--- a/solution.py
+++ b/solution.py
@@ -414,6 +414,7 @@
         entry_parts(range(seqs + 1, 2 * seqs), r)
     with scope("earr_last"):
         entry_arrived(last)
+    forwards(1, 0, edge)
 
     def halo(pair, i):
         ref = (cbuf, pbuf)[i]
@@ -428,7 +429,6 @@
             launch(halo(pair, i), sp < n - 1)
     for s in own[1:]:
         launch(shift_copy(s))
-    forwards(1, 0, edge)
     forwards(3, 0, inner)
 
     def halo_wait(pair):
@@ -655,10 +655,12 @@
         start_copy.wait_recv()
     fix(PEER, 0)
     lead = own_units[:2] + peer_units[:1] + own_units[2:3]
-    for c in lead:
+    for c in lead[:2]:
+        peer_step(pl.ds(0, 1), c)
+    forwards(3, 0, edge)
+    for c in lead[2:]:
         peer_step(pl.ds(0, 1), c)
     flush()
-    forwards(3, 0, edge)
     for s0 in later:
         with scope(f"shift_wait#s={s0}"):
             shift_copy(s0).wait_recv()
@@ -681,13 +683,12 @@
     for c in peer_units[1:2]:
         peer_step(every, c)
     forwards(3, 1, edge)
-    fix(OWN, 0)
     flush()
     for s0 in later:
         chain(OWN, s0)
     for c in peer_units[2:3]:
         peer_step(every, c)
-    for s0 in later:
+    for s0 in own:
         fix(OWN, s0)
     for c in lead[:2]:
         dots(OWN, every, c)

time: 115 us -> 112 us (0.974)
  the two profiles are of different devices: /device:TPU:0 before, /device:TPU:25 now
where the time goes in v4:
time: 112 us
  Pallas kernels  111 us (99%)
  local copies, waits for them, and re-layouts  1.15 us (1%)
    pallas_call x1, Pallas kernels, per_device(): pl.pallas_call(functools.partial(kernel, n, m), name='layer', out_shape=p...  111 us

profile of v4, /device:TPU:25, one launch (start us, length us, event | category | flops | bytes accessed | tf_op | source)
XLA Modules:
  0.0 112.0 jit_solution(302018916400110992)
XLA Ops:
  0.0 110.9 %layer.1 = bf16[2,192,2048]{2,1,0:T(8,128)(2,1)S(1)} custom-call(bf16[2,192,2048]{2,1,0:T(8,128)(2,1)} %tokens.1, f32[1,2048]{1,0:T(1,128)} %bitcast.3, bf16[128,1024]{1,0:T(8,128)(2,1)} %chain_entry.1, bf16[128,1024]{1,0:T(8,128)(2,1)} %pool_entry.1, bf16[4,1024]{1,0:T(4,128)(2,1)} %taps.1, bf16[4,256,256]{2,1,0:T(8,128)(2,1)} %rgate.1, ...), custom_call_target="tpu_custom_call" | custom-call | tf_op jit(solution)/shard_map/layer/pallas_call | solution.py:767
  110.9 1.1 %copy.16 = bf16[2,192,2048]{2,1,0:T(8,128)(2,1)} copy(bf16[2,192,2048]{2,1,0:T(8,128)(2,1)S(1)} %layer.1) | data formatting | bytes 3145728
